TPU v7x, 128 devices: a whole 4x4x4 slice. The times are simulated.
128 devices in a mesh: sp: 16 (over z, x), tp: 8 (over y, core).
Axes of the slice: x: 4, y: 4, z: 4, core: 2. Of those that a mesh axis runs over, the one named last changes fastest.
Arguments:
- queries: bfloat16 [16384, 1536], P('sp', 'tp'), may hold values from -200 to 200
- key_heads: bfloat16 [16384, 512], P('sp', 'tp'), may hold values from -6 to 6
- projected_value_heads: bfloat16 [16384, 512], P('sp', 'tp'), may hold values from -5 to 5
- sink_logit_table: float32 [24], P('tp'), may hold values from 0 to 4
- out_weight: bfloat16 [1536, 3072], P('tp'), may hold values from -1.5 to 1.5
- residual: bfloat16 [16384, 3072], P('sp', 'tp'), may hold values from -16 to 16
- norm_gain: bfloat16 [3072], P('tp'), may hold values from 0.099609375 to 1.8984375
- up_weight: bfloat16 [3072, 12288], P('sp', 'tp'), may hold values from -0.109375 to 0.109375
- down_weight: bfloat16 [12288, 3072], P('tp', 'sp'), may hold values from -0.0546875 to 0.0546875
Outputs:
- result: bfloat16 [16384, 3072], P('sp', 'tp')
All inputs are finite; a program needn't handle non-finite values.
Results may differ from a plain program's by a relative error of at most 0.015.
Values may be sent and summed in bfloat16 or wider, within the bound.
A program may use at most 128 MiB of HBM per device.

v0:
```python
import jax
import jax.numpy as jnp
from jax import lax
from jax.sharding import PartitionSpec as P

D = 3072
HEAD_SIZE = 64
WINDOW_SPAN = 128


epsilon = 1e-06


def turned_gather(arrays, axis, dims):
    turned = [jnp.moveaxis(a, dim, 0) for a, dim in zip(arrays, dims)]
    both = jnp.concatenate([t.reshape(len(t), -1) for t in turned], axis=1)
    result, at, done = (lax.all_gather(both, axis, axis=0, tiled=True), 0, [])
    for t, dim in zip(turned, dims):
        piece = result[:, at : at + t[0].size].reshape(-1, *t.shape[1:])
        done.append(jnp.moveaxis(piece, 0, dim))
        at += t[0].size
    return tuple(done)


def shifted(block, axis, distance):
    devices = range(lax.axis_size(axis))
    route = [(i - distance, i) for i in devices if i - distance in devices]
    return lax.ppermute(block, axis, route)


def from_everyone(x, axis):
    copies = jnp.broadcast_to(x, (lax.axis_size(axis), *x.shape))
    return lax.all_to_all(copies, axis, split_axis=0, concat_axis=0, tiled=True)


def over_copies(x, axis):
    everything = from_everyone(x, axis)
    return jnp.sum(everything, axis=0)


def in_order(pieces, dim):
    pieces = jnp.moveaxis(pieces, 0, dim)
    shape = pieces.shape
    return pieces.reshape(*shape[:dim], shape[dim] * shape[dim + 1], *shape[dim + 2 :])


def gathered_copies(x, axis, dim):
    pieces = from_everyone(x, axis)
    return in_order(pieces, dim)


def attend(queries, key_heads, projected_value_heads, sink_logit_table, previous, offset):
    row_count = queries.shape[0]
    kv_cols = key_heads.shape[1]
    kv_local = kv_cols // HEAD_SIZE
    group_count = queries.shape[1] // kv_cols
    block_count = row_count // WINDOW_SPAN
    extended_keys = jnp.concatenate([previous[:, :kv_cols], key_heads], axis=0)
    extended_values = jnp.concatenate([previous[:, kv_cols:], projected_value_heads], axis=0)

    def banded(source_rows):
        shaped = source_rows.reshape(block_count + 1, WINDOW_SPAN, kv_local, HEAD_SIZE)
        return jnp.concatenate([shaped[:-1], shaped[1:]], axis=1)

    key_band = banded(extended_keys)
    value_band = banded(extended_values)
    query_block_list = queries.reshape(block_count, WINDOW_SPAN, kv_local, group_count, HEAD_SIZE)
    scores = jnp.einsum(
        "nqkgd,nskd->nkgqs", query_block_list, key_band, preferred_element_type=jnp.float32
    ) * HEAD_SIZE ** (-0.5)
    within = jnp.arange(WINDOW_SPAN)[:, None]
    column = jnp.arange(2 * WINDOW_SPAN)[None, :]
    distance = WINDOW_SPAN + within - column
    valid = (distance >= 0) & (distance < WINDOW_SPAN)
    key_pos = (
        offset
        + jnp.arange(block_count)[:, None] * WINDOW_SPAN
        + jnp.arange(2 * WINDOW_SPAN)[None, :]
        - WINDOW_SPAN
    )
    allowed = valid[None] & (key_pos >= 0)[:, None, :]
    allowed = allowed[:, None, None]
    head_sink_logit = sink_logit_table.reshape(kv_local, group_count)[None, :, :, None, None]
    masked = jnp.where(allowed, scores, -1e30)
    ceiling = jnp.maximum(jnp.max(masked, axis=-1, keepdims=True), head_sink_logit)
    powers = jnp.where(allowed, jnp.exp(masked - ceiling), 0.0)
    denom = jnp.sum(powers, axis=-1, keepdims=True) + jnp.exp(head_sink_logit - ceiling)
    probs = (powers / denom).astype(jnp.bfloat16)
    output = jnp.einsum("nkgqs,nskd->nqkgd", probs, value_band, preferred_element_type=jnp.float32)
    return output.astype(jnp.bfloat16).reshape(row_count, queries.shape[1])


def rounded(values):
    return lax.optimization_barrier(values.astype(jnp.bfloat16)).astype(jnp.float32)


def body(
    queries,
    key_heads,
    projected_value_heads,
    sink_logit_table,
    out_weight,
    residual,
    norm_gain,
    up_weight,
    down_weight,
):
    row_count = queries.shape[0]
    offset = lax.axis_index("sp") * row_count
    up_whole, down_whole = turned_gather((up_weight, down_weight), "sp", (0, 1))
    tail = jnp.concatenate(
        [key_heads[row_count - WINDOW_SPAN :], projected_value_heads[row_count - WINDOW_SPAN :]],
        axis=1,
    )
    previous = shifted(tail, "sp", 1)
    attended = attend(queries, key_heads, projected_value_heads, sink_logit_table, previous, offset)
    partial_value = rounded(jnp.dot(attended, out_weight, preferred_element_type=jnp.float32))
    mixed_sum = lax.psum_scatter(
        partial_value.astype(jnp.bfloat16), "tp", scatter_dimension=1, tiled=True
    ).astype(jnp.float32)
    stream = rounded(residual.astype(jnp.float32) + mixed_sum)
    squares = over_copies(jnp.sum(stream * stream, axis=1, keepdims=True), "tp")
    normed = (stream * lax.rsqrt(squares / D + epsilon) * norm_gain.astype(jnp.float32)).astype(
        jnp.bfloat16
    )
    normed_whole = gathered_copies(normed, "tp", 1)
    hidden_pre = jnp.dot(normed_whole, up_whole, preferred_element_type=jnp.float32)
    activated = jnp.square(jax.nn.relu(hidden_pre)).astype(jnp.bfloat16)
    terms = jnp.dot(activated, down_whole, preferred_element_type=jnp.float32)
    branch_sum = lax.psum_scatter(
        rounded(terms).astype(jnp.bfloat16), "tp", scatter_dimension=1, tiled=True
    ).astype(jnp.float32)
    return (stream + branch_sum).astype(jnp.bfloat16)


def solution(mesh):
    return jax.shard_map(
        body,
        mesh=mesh,
        in_specs=(
            P("sp", "tp"),
            P("sp", "tp"),
            P("sp", "tp"),
            P("tp"),
            P("tp", None),
            P("sp", "tp"),
            P("tp"),
            P("sp", "tp"),
            P("tp", "sp"),
        ),
        out_specs=P("sp", "tp"),
        check_vma=False,
    )
```

profile of v0, /device:TPU:9, one launch (start us, length us, event | category | flops | bytes accessed | tf_op | source)
XLA Modules:
  0.0 255.4 jit_solution(14441253247920430598)
XLA Ops:
  7.4 0.0 copy-start
  7.4 0.0 reduce-scatter.7.cloned.1.call-start
  7.4 0.8 slice.38
  8.2 0.7 slice.39
  8.9 3.1 %collective-permute-start = (bf16[128,128]{0,1:T(8,128)(2,1)S(1)}, bf16[128,128]{0,1:T(8,128)(2,1)S(1)}, u32[]{:S(2)}, u32[]{:S(2)}) collective-permute-start(bf16[128,128]{0,1:T(8,128)(2,1)S(1)} %pad_maximum_fusion.3), channel_id=1, source_target_pairs={{0,8},{8,16},{16,24},{24,32},{32,40},{40,48},{48,56},{56,64},{64,7... | collective-permute-start | bytes 98312 | tf_op jit(solution)/shard_map/ppermute | solution.py:28
  12.1 0.1 add_compare_fusion
  12.2 0.3 broadcast_and_fusion
  12.5 1.1 copy.39
  13.6 0.9 copy.38
  14.5 0.0 copy-start.5
  14.6 0.9 copy.36
  15.5 0.0 collective-permute-done
  15.5 1.0 fusion.32
  16.6 0.7 fusion.9
  17.2 0.0 copy-done.5
  17.3 0.1 broadcast_maximum_fusion
  17.3 0.9 fusion.10
  18.2 0.1 exponential_add_fusion
  18.3 1.1 fusion.21
  19.4 0.3 copy.26
  19.6 0.0 copy-done
  19.7 4.5 %convolution_convert_fusion = bf16[1024,3072]{1,0:T(8,128)(2,1)} fusion(bf16[192,3072]{1,0:T(8,128)(2,1)S(1)} %copy-done, bf16[24,8,8,128]{3,2,1,0:T(8,128)(2,1)S(1)} %bitcast.92), kind=kOutput, calls=%fused_computation.6 | convolution fusion | flops 1211105280 | bytes 7864320 | tf_op jit(solution)/shard_map/dot_general | solution.py:117
  24.1 8.7 %copy.31 = bf16[1024,3072]{0,1:T(8,128)(2,1)} copy(bf16[1024,3072]{1,0:T(8,128)(2,1)} %convolution_convert_fusion) | data formatting | bytes 12582912
  32.8 0.0 copy-start.3
  32.8 0.0 copy-start.4
  32.8 0.0 reduce-scatter.7.cloned.1.call-update
  32.9 0.0 copy-start.2
  32.9 0.0 all-gather.2.cloned.1.call-start
  32.9 1.0 copy-done.3
  33.9 0.2 copy-done.4
  34.1 1.2 pad_maximum_fusion
  35.3 0.0 copy-start.6
  35.3 0.0 all-gather.2.cloned.1.call-update
  35.4 41.6 %reduce-scatter.7.cloned.1.call-done = bf16[384,1024]{1,0:T(8,128)(2,1)} async-done(((bf16[3072,1024]{1,0:T(8,128)(2,1)}), bf16[384,1024]{1,0:T(8,128)(2,1)}) %reduce-scatter.7.cloned.1.call-update) | async-done | bytes 786448
  77.0 1.5 copy.32
  78.4 0.0 copy-done.2
  78.5 0.2 add_convert_fusion
  78.7 0.2 fusion.11
  78.9 0.6 broadcast_in_dim.38
  79.5 5.8 %all-to-all-start = ((f32[8,1024,1]{1,2,0:T(1,128)}), f32[8,1024,1]{1,2,0:T(1,128)S(1)}, u32[]{:S(2)}, u32[]{:S(2)}) async-start(f32[8,1024,1]{1,2,0:T(1,128)} %broadcast_in_dim.38), calls=%async_computation | async-start | bytes 65536 | tf_op jit(solution)/shard_map/all_to_all | solution.py:33
  85.4 0.0 reduce-scatter.9.cloned.1.call-start
  85.4 0.0 copy-done.6
  85.4 4.1 %all-to-all-done = f32[8,1024,1]{1,2,0:T(1,128)S(1)} async-done(((f32[8,1024,1]{1,2,0:T(1,128)}), f32[8,1024,1]{1,2,0:T(1,128)S(1)}, u32[]{:S(2)}, u32[]{:S(2)}) %all-to-all-start) | async-done | bytes 32800 | tf_op jit(solution)/shard_map/all_to_all | solution.py:33
  89.5 0.3 fusion.13
  89.8 0.3 copy.27
  90.1 0.8 broadcast_in_dim.39
  90.9 75.6 %all_to_all.10 = bf16[8,1024,384]{1,2,0:T(8,128)(2,1)} all-to-all(bf16[8,1024,384]{1,2,0:T(8,128)(2,1)S(1)} %broadcast_in_dim.39), channel_id=1, replica_groups=mesh['sp'=16,'tp'=8] {'tp'}, dimensions={0} | all-to-all | bytes 12582912 | tf_op jit(solution)/shard_map/all_to_all | solution.py:33
  166.5 0.0 all-gather.2.cloned.1.call-done
  166.5 14.1 %multiply_convert_fusion = bf16[1024,1536]{1,0:T(8,128)(2,1)S(1)} fusion(bf16[1024,3072]{0,1:T(8,128)(2,1)} %bitcast.91, bf16[3072,3072]{1,0:T(8,128)(2,1)} %all-gather.2.cloned.1.call-done), kind=kOutput, calls=%fused_computation.4 | convolution fusion | flops 9668395008 | bytes 18874368 | tf_op jit(solution)/shard_map/dot_general | solution.py:127
  180.7 14.3 %fusion.4 = bf16[1024,3072]{1,0:T(8,128)(2,1)} fusion(bf16[1024,1536]{1,0:T(8,128)(2,1)S(1)} %multiply_convert_fusion, bf16[3072,3072]{1,0:T(8,128)(2,1)} %all-gather.2.cloned.1.call-done), kind=kOutput, calls=%fused_computation.5 | convolution fusion | flops 9666822144 | bytes 18874368 | tf_op jit(solution)/shard_map/dot_general | solution.py:129
  195.0 8.6 %copy.33 = bf16[1024,3072]{0,1:T(8,128)(2,1)} copy(bf16[1024,3072]{1,0:T(8,128)(2,1)} %fusion.4) | data formatting | bytes 12582912
  203.6 0.0 reduce-scatter.9.cloned.1.call-update
  203.6 0.0 copy-start.1
  203.6 41.7 %reduce-scatter.9.cloned.1.call-done = bf16[384,1024]{1,0:T(8,128)(2,1)} async-done(((bf16[3072,1024]{1,0:T(8,128)(2,1)}), bf16[384,1024]{1,0:T(8,128)(2,1)}) %reduce-scatter.9.cloned.1.call-update) | async-done | bytes 786448
  245.4 1.5 copy.34
  246.8 1.1 fusion.14
  247.9 0.0 copy-done.1
  (14 shorter events, 0.2 us)
Async XLA Ops:
  7.4 12.3 %copy-start = (bf16[192,3072]{1,0:T(8,128)(2,1)S(1)}, bf16[192,3072]{1,0:T(8,128)(2,1)}, u32[]{:S(2)}) copy-start(bf16[192,3072]{1,0:T(8,128)(2,1)} %param.13) | copy-start | bytes 3538948
  7.4 69.6 %reduce-scatter.7.cloned.1.call-start = ((), (), s32[]{:S(2)}) async-start(), calls=%async_computation.5 | async-start | bytes 7077888
  8.9 6.6 %collective-permute-start = (bf16[128,128]{0,1:T(8,128)(2,1)S(1)}, bf16[128,128]{0,1:T(8,128)(2,1)S(1)}, u32[]{:S(2)}, u32[]{:S(2)}) collective-permute-start(bf16[128,128]{0,1:T(8,128)(2,1)S(1)} %pad_maximum_fusion.3), channel_id=1, source_target_pairs={{0,8},{8,16},{16,24},{24,32},{32,40},{40,48},{48,56},{56,64},{64,7... | collective-permute-start | bytes 98312 | tf_op jit(solution)/shard_map/ppermute | solution.py:28
  14.5 2.7 %copy-start.5 = (f32[3]{0:T(128)S(1)}, f32[3]{0:T(128)}, u32[]{:S(2)}) copy-start(f32[3]{0:T(128)} %param.12) | copy-start | bytes 40
  32.8 1.1 copy-start.3
  32.8 1.2 copy-start.4
  32.9 45.6 %copy-start.2 = (bf16[1024,384]{1,0:T(8,128)(2,1)S(1)}, bf16[1024,384]{1,0:T(8,128)(2,1)}, u32[]{:S(2)}) copy-start(bf16[1024,384]{1,0:T(8,128)(2,1)} %param.14) | copy-start | bytes 2359300
  32.9 133.6 %all-gather.2.cloned.1.call-start = ((), (), s32[]{:S(2)}) async-start(), calls=%async_computation.4 | async-start | bytes 20054016 | tf_op jit(solution)/shard_map/all_gather | solution.py:17
  35.3 50.1 %copy-start.6 = (bf16[384]{0:T(512)(128)(2,1)S(1)}, bf16[384]{0:T(512)(128)(2,1)}, u32[]{:S(2)}) copy-start(bf16[384]{0:T(512)(128)(2,1)} %param.15) | copy-start | bytes 2308
  79.5 9.9 %all-to-all-start = ((f32[8,1024,1]{1,2,0:T(1,128)}), f32[8,1024,1]{1,2,0:T(1,128)S(1)}, u32[]{:S(2)}, u32[]{:S(2)}) async-start(f32[8,1024,1]{1,2,0:T(1,128)} %broadcast_in_dim.38), calls=%async_computation | async-start | bytes 65536 | tf_op jit(solution)/shard_map/all_to_all | solution.py:33
  85.4 160.0 %reduce-scatter.9.cloned.1.call-start = ((), (), s32[]{:S(2)}) async-start(), calls=%async_computation.6 | async-start | bytes 7077888
  203.6 44.3 %copy-start.1 = (bf16[192,3072]{1,0:T(8,128)(2,1)S(1)}, bf16[192,3072]{1,0:T(8,128)(2,1)}, u32[]{:S(2)}) copy-start(bf16[192,3072]{1,0:T(8,128)(2,1)} %param.13) | copy-start | bytes 3538948
Sparse Core Ops, SparseCore 0:
  33.0 43.9 reduce-scatter.6
  203.7 41.5 reduce-scatter.8
Sparse Core Ops, SparseCore 1:
  35.5 124.0 all-gather.1
where the time goes:
time: 257 us; the launch traced here: 255 us
  waiting for transfers between devices  87.4 us (34%)
  blocking collectives  75.6 us (29%)
  matrix products  34.6 us (13%)
  local copies, waits for them, and re-layouts  28.1 us (11%)
  between operations  15.1 us (6%)
  starting transfers between devices  8.99 us (3%)
  other arithmetic  5.53 us (2%)
    unnamed x5, waiting for transfers between devices  83.4 us
    all_to_all x1, blocking collectives, from_everyone(): return lax.all_to_all(copies, axis, split_axis=0, concat_axis=0, tiled=True)  75.6 us
    unnamed x23, local copies, waits for them, and re-layouts  24.4 us
    dot_general x1, matrix products, body(): terms = jnp.dot(activated, down_whole, preferred_element_type=jnp.float32)  14.3 us
    dot_general x1, matrix products, body(): jnp.dot(normed_whole, up_whole, preferred_element_type=jnp.float32)  14.1 us
    all_to_all x1, starting transfers between devices, from_everyone(): return lax.all_to_all(copies, axis, split_axis=0, concat_axis=0, tiled=True)  5.83 us
  transfers between devices with their start and end apart: 5, of which 3 were waited for; matrix products, arithmetic and copies ran while one was open for 3% of the time, Pallas kernels for 0%

commit v1 on v0

v1 whole, which is shorter than its diff:
```python
import functools

import jax
import jax.numpy as jnp
from jax import lax
from jax.experimental import pallas as pl
from jax.experimental.pallas import tpu as pltpu
from jax.sharding import PartitionSpec as P

D = 3072
HEAD_SIZE = 64
WINDOW = 128
EPSILON = 1e-06

ROWS = 1024
FEATURES = 384
HEADS = 192
SHARD = 192
HALF = 96
QUARTER = 48
HIDDEN = 1536
TILE = 256

MESH = pl.DeviceIdType.MESH
BF16 = jnp.bfloat16
F32 = jnp.float32


def dot(a, b, dims):
    return lax.dot_general(a, b, (dims, ((), ())), preferred_element_type=F32)


def kernel(
    queries, keys, values, sink, out_weight, residual, gain, up, down,
    result,
    up_all, down_all, x_all, att_all, w_all, hidden, act, mixed, stream, res_v,
    q_v, k_v, v_v, halo_k, halo_v, partials, paired, chained, final, squares, inverse, out_v,
    local_sem, w_send, w_recv, halo_send, halo_recv, g_send, g_recv,
    att_send, att_recv, x_send, x_recv, sq_send, sq_recv,
    pair_send, pair_recv, chain_send, chain_recv, final_send, final_recv,
):
    s, t = lax.axis_index("sp"), lax.axis_index("tp")
    z, x = s // 4, s % 4
    y, c = t // 2, t % 2

    def ring(position, by):
        return (position + by + 4) % 4

    def device(zz, xx, yy, cc):
        return (zz * 4 + xx, yy * 2 + cc)

    partner = (s, y * 2 + (1 - c))
    y_next = {1: (s, ring(y, 1) * 2 + c), -1: (s, ring(y, -1) * 2 + c)}
    DIRS = ((0, 1), (1, -1))

    def remote(src, dst, send, recv, target):
        return pltpu.make_async_remote_copy(
            src_ref=src, dst_ref=dst, send_sem=send, recv_sem=recv,
            device_id=target, device_id_type=MESH,
        )

    pending = []

    def start(copy):
        copy.start()
        pending.append(copy)

    barrier = pltpu.get_barrier_semaphore()
    greeted = [
        device(z, ring(x, 1), y, c), device(z, ring(x, -1), y, c),
        device(ring(z, 1), x, y, c), device(ring(z, -1), x, y, c),
        ((s + 1) % 16, t), ((s + 15) % 16, t),
    ] + [(s, (t + k) % 8) for k in range(1, 8)]
    for other in greeted:
        pl.semaphore_signal(barrier, inc=1, device_id=other, device_id_type=MESH)
    locals_ = [
        pltpu.make_async_copy(src, dst, local_sem.at[i])
        for i, (src, dst) in enumerate([
            (queries, q_v), (keys, k_v), (values, v_v), (residual, res_v),
            (up, up_all.at[pl.ds(pl.multiple_of(s * SHARD, SHARD), SHARD)]),
            (down, down_all.at[pl.ds(pl.multiple_of(s * SHARD, SHARD), SHARD)]),
            (out_weight.at[:, pl.ds(pl.multiple_of(t * FEATURES, 128), FEATURES)],
             w_all.at[pl.ds(pl.multiple_of(t * HEADS, HEADS), HEADS)]),
        ])
    ]
    for copy in locals_:
        copy.start()
    pl.semaphore_wait(barrier, len(greeted))

    STEPS = (0, -1, 1, 2)

    class Gather:
        def __init__(self, own, buf, base):
            self.own, self.buf, self.base = own, buf, base

        def spot(self, half, sec, prim, low, count):
            zz, xx = (sec, prim) if half == 0 else (prim, sec)
            row = (zz * 4 + xx) * SHARD + half * HALF + low
            return self.buf.at[pl.ds(pl.multiple_of(row, 16), count)]

        def copy(self, half, index, src, dst, target):
            k = self.base + half * 20 + index
            return remote(src, dst, g_send.at[k], g_recv.at[k], target)

        def at(self, half):
            return (z, x) if half == 0 else (x, z)

        def towards(self, half, primary, by):
            if primary == (half == 0):
                return device(z, ring(x, by), y, c)
            return device(ring(z, by), x, y, c)

        def first(self):
            for half in (0, 1):
                sec, prim = self.at(half)
                src = self.own.at[pl.ds(half * HALF, HALF)]
                dst = self.spot(half, sec, prim, 0, HALF)
                for d, by in DIRS:
                    start(self.copy(half, d, src, dst, self.towards(half, True, by)))
            for half in (0, 1):
                sec, prim = self.at(half)
                src = self.own.at[pl.ds(half * HALF, HALF)]
                dst = self.spot(half, sec, prim, 0, HALF)
                for d, by in DIRS:
                    start(self.copy(half, 4 + d, src, dst, self.towards(half, False, by)))

        def wait(self, half, index, sec, prim, low, count):
            ref = self.spot(half, sec, prim, low, count)
            self.copy(half, index, ref, ref, partner).wait_recv()

        def second(self):
            for half in (0, 1):
                sec, prim = self.at(half)
                for d, by in DIRS:
                    origin = ring(prim, -by)
                    self.wait(half, d, sec, origin, 0, HALF)
                    piece = self.spot(half, sec, origin, d * QUARTER, QUARTER)
                    start(self.copy(half, 2 + d, piece, piece, self.towards(half, True, by)))
            for half in (0, 1):
                for j in (1, 2):
                    self.spread(half, j)

        def spread(self, half, j):
            sec, prim = self.at(half)
            piece = self.spot(half, sec, ring(prim, STEPS[j]), 0, HALF)
            for d, by in DIRS:
                start(self.copy(half, 4 + 2 * j + d, piece, piece, self.towards(half, False, by)))

        def third(self):
            for half in (0, 1):
                sec, prim = self.at(half)
                for d, by in DIRS:
                    self.wait(half, 2 + d, sec, ring(prim, 2), d * QUARTER, QUARTER)
                self.spread(half, 3)

        def forward(self, j):
            for half in (0, 1):
                sec, prim = self.at(half)
                origin = ring(prim, STEPS[j])
                for d, by in DIRS:
                    self.wait(half, 4 + 2 * j + d, ring(sec, -by), origin, 0, HALF)
                    piece = self.spot(half, ring(sec, -by), origin, d * QUARTER, QUARTER)
                    start(self.copy(half, 12 + 2 * j + d, piece, piece, self.towards(half, False, by)))

        def last(self, j):
            for half in (0, 1):
                sec, prim = self.at(half)
                origin = ring(prim, STEPS[j])
                for d, by in DIRS:
                    self.wait(half, 12 + 2 * j + d, ring(sec, 2), origin, d * QUARTER, QUARTER)

    up_gather = Gather(up, up_all, 0)
    down_gather = Gather(down, down_all, 40)
    up_gather.first()

    after = ((s + 1) % 16, t)
    tail = pl.ds(ROWS - WINDOW, WINDOW)
    halo_copies = [
        remote(keys.at[:, tail], halo_k, halo_send.at[0], halo_recv.at[0], after),
        remote(values.at[:, tail], halo_v, halo_send.at[1], halo_recv.at[1], after),
    ]
    for copy in halo_copies:
        start(copy)
    w_mine = w_all.at[pl.ds(pl.multiple_of(t * HEADS, HEADS), HEADS)]
    w_copies = []
    for k in range(1, 8):
        owner = (t + k) % 8
        copy = remote(
            out_weight.at[:, pl.ds(pl.multiple_of(owner * FEATURES, 128), FEATURES)],
            w_mine, w_send.at[k - 1], w_recv.at[k - 1], (s, owner),
        )
        start(copy)
        w_copies.append(copy)

    sinks = jnp.concatenate([jnp.full((1, WINDOW), sink[g], F32) for g in range(3)], axis=1)
    key_at = lax.broadcasted_iota(jnp.int32, (2 * WINDOW, 3 * WINDOW), 0)
    query_at = lax.broadcasted_iota(jnp.int32, (2 * WINDOW, 3 * WINDOW), 1) % WINDOW
    mine_row = t * HEADS

    def attend(n, key_band, value_band, allowed):
        lanes = pl.ds(pl.multiple_of(n * WINDOW, WINDOW), WINDOW)
        q = jnp.concatenate([q_v[pl.ds(g * HEAD_SIZE, HEAD_SIZE), lanes] for g in range(3)], axis=1)
        scores = dot(key_band, q, ((0,), (0,))) * HEAD_SIZE**-0.5
        masked = jnp.where(allowed, scores, -1e30)
        top = jnp.maximum(jnp.max(masked, axis=0, keepdims=True), sinks)
        powers = jnp.where(allowed, jnp.exp(masked - top), 0.0)
        denom = jnp.sum(powers, axis=0, keepdims=True) + jnp.exp(sinks - top)
        probs = (powers * (1.0 / denom)).astype(BF16)
        output = dot(value_band, probs, ((1,), (0,))).astype(BF16)
        for g in range(3):
            rows = pl.ds(pl.multiple_of(mine_row + g * HEAD_SIZE, HEAD_SIZE), HEAD_SIZE)
            att_all[rows, lanes] = output[:, g * WINDOW : (g + 1) * WINDOW]

    near = (key_at > query_at) & (key_at <= query_at + WINDOW)
    for copy in locals_[:3]:
        copy.wait()

    @pl.loop(1, 8)
    def _(n):
        band = pl.ds(pl.multiple_of((n - 1) * WINDOW, WINDOW), 2 * WINDOW)
        attend(n, k_v[:, band], v_v[:, band], near)

    for copy in halo_copies:
        copy.wait_recv()
    first_key = jnp.where(s == 0, WINDOW, 0)
    attend(
        0,
        jnp.concatenate([halo_k[...], k_v[:, 0:WINDOW]], axis=1),
        jnp.concatenate([halo_v[...], v_v[:, 0:WINDOW]], axis=1),
        near & (key_at >= first_key),
    )

    def att_rows(yy, cc, low=0, count=HEADS):
        row = (yy * 2 + cc) * HEADS + low
        return att_all.at[pl.ds(pl.multiple_of(row, 32), count)]

    def att_copy(index, ref, target):
        return remote(ref, ref, att_send.at[index], att_recv.at[index], target)

    def att_arrived(index, ref):
        att_copy(index, ref, partner).wait_recv()

    for d, by in DIRS:
        start(att_copy(d, att_rows(y, c), y_next[by]))
    start(att_copy(4, att_rows(y, c), partner))
    up_gather.second()

    for i, copy in enumerate(locals_[3:]):
        copy.wait()
    for copy in w_copies:
        copy.wait_recv()

    def mix(yy, first):
        rows = pl.ds(pl.multiple_of(yy * 2 * HEADS, 2 * HEADS), 2 * HEADS)

        @pl.loop(0, ROWS // TILE)
        def _(i):
            tokens = pl.ds(pl.multiple_of(i * TILE, TILE), TILE)
            part = dot(att_all[rows, tokens], w_all[rows, :], ((0,), (0,)))
            mixed[tokens, :] = part if first else mixed[tokens, :] + part

    att_arrived(4, att_rows(y, 1 - c))
    mix(y, True)
    for d, by in DIRS:
        att_arrived(d, att_rows(ring(y, -by), c))
        start(att_copy(2 + d, att_rows(ring(y, -by), c, d * HALF, HALF), y_next[by]))
        start(att_copy(5 + d, att_rows(ring(y, -by), c), partner))
    up_gather.third()
    for d, by in DIRS:
        att_arrived(5 + d, att_rows(ring(y, -by), 1 - c))
        mix(ring(y, -by), False)
    for d, by in DIRS:
        att_arrived(2 + d, att_rows(ring(y, 2), c, d * HALF, HALF))
    start(att_copy(7, att_rows(ring(y, 2), c), partner))
    att_arrived(7, att_rows(ring(y, 2), 1 - c))
    mix(ring(y, 2), False)

    lanes_of = lambda cc: pl.ds(pl.multiple_of(cc * FEATURES, 128), FEATURES)

    def x_block(yy, cc, low=0, count=ROWS):
        return x_all.at[pl.ds(pl.multiple_of(yy * ROWS + low, 512), count), lanes_of(cc)]

    gains = gain[...].astype(F32)
    ones = jnp.ones((8, FEATURES), BF16)
    sq_rows = pl.ds(pl.multiple_of(t * 8, 8), 8)

    @pl.loop(0, ROWS // TILE)
    def _(i):
        tokens = pl.ds(pl.multiple_of(i * TILE, TILE), TILE)
        here = (res_v[tokens, :].astype(F32) + mixed[tokens, :]).astype(BF16)
        stream[tokens, :] = here
        wide = here.astype(F32)
        x_all[pl.ds(pl.multiple_of(y * ROWS + i * TILE, TILE), TILE), lanes_of(c)] = (wide * gains).astype(BF16)
        sq = wide * wide
        high = sq.astype(BF16)
        low = (sq - high.astype(F32)).astype(BF16)
        squares[sq_rows, tokens] = dot(ones, high, ((1,), (1,))) + dot(ones, low, ((1,), (1,)))

    def x_copy(index, ref, target):
        return remote(ref, ref, x_send.at[index], x_recv.at[index], target)

    def x_arrived(index, ref):
        x_copy(index, ref, partner).wait_recv()

    for part in (0, 1):
        for d, by in DIRS:
            start(x_copy(2 * part + d, x_block(y, c, part * 512, 512), y_next[by]))
    start(x_copy(6, x_block(y, c), partner))
    sq_copies = []
    for k in range(1, 8):
        ref = squares.at[sq_rows]
        copy = remote(ref, ref, sq_send.at[k - 1], sq_recv.at[k - 1], (s, (t + k) % 8))
        start(copy)
        sq_copies.append(copy)

    up_gather.forward(0)
    up_gather.forward(1)
    up_gather.forward(2)
    x_arrived(0, x_block(ring(y, -1), c, 0, 512))
    start(x_copy(4, x_block(ring(y, -1), c, 0, 512), y_next[1]))
    x_arrived(1, x_block(ring(y, 1), c, 0, 512))
    up_gather.forward(3)
    down_gather.first()
    x_arrived(3, x_block(ring(y, 1), c, 512, 512))
    start(x_copy(5, x_block(ring(y, 1), c, 512, 512), y_next[-1]))
    x_arrived(2, x_block(ring(y, -1), c, 512, 512))
    start(x_copy(7, x_block(ring(y, -1), c), partner))
    start(x_copy(8, x_block(ring(y, 1), c), partner))

    def hide(yy, first, last):
        @pl.loop(0, ROWS // TILE)
        def _(i):
            tokens = pl.ds(pl.multiple_of(i * TILE, TILE), TILE)
            block = x_all[pl.ds(pl.multiple_of(yy * ROWS + i * TILE, TILE), TILE), :]
            for n in range(3):
                cols = pl.ds(n * 512, 512)
                part = dot(block, up_all[pl.ds(pl.multiple_of(yy * 768, 768), 768), cols], ((1,), (0,)))
                if not first:
                    part = part + hidden[tokens, cols]
                if last:
                    act[tokens, cols] = jnp.square(jnp.maximum(part, 0.0)).astype(BF16)
                else:
                    hidden[tokens, cols] = part

    for j in range(4):
        up_gather.last(j)
    x_arrived(6, x_block(y, 1 - c))
    hide(y, True, False)
    for d, by in DIRS:
        x_arrived(7 + d, x_block(ring(y, -by), 1 - c))
        hide(ring(y, -by), False, False)
    x_arrived(4, x_block(ring(y, 2), c, 0, 512))
    x_arrived(5, x_block(ring(y, 2), c, 512, 512))
    start(x_copy(9, x_block(ring(y, 2), c), partner))
    down_gather.second()
    x_arrived(9, x_block(ring(y, 2), 1 - c))
    hide(ring(y, 2), False, True)

    for copy in sq_copies:
        copy.wait_recv()
    total = jnp.zeros((1, ROWS), F32)
    for k in range(8):
        total = total + squares[pl.ds(8 * k, 1), :]
    factor = 1.0 / (total * (1.0 / D) + EPSILON)
    inverse[...] = jnp.transpose(jnp.broadcast_to(factor, (128, ROWS)))

    own_pair = x // 2
    BLOCKS = ((0, 0), (0, 1), (0, 2), (1, 0), (0, 3), (1, 1), (1, 2), (1, 3))
    SHIFT = (0, 1, -1, 2)

    def slot(kind, j):
        return pl.ds(pl.multiple_of((kind * 4 + j) * ROWS, ROWS), ROWS)

    def pair_slot(j):
        return pl.ds(pl.multiple_of(j * ROWS, ROWS), ROWS)

    def facts(kind, j):
        pair = own_pair if kind == 0 else 1 - own_pair
        owner = ring(z, SHIFT[j])
        return pair, owner, c == pair, (y - owner + 4) % 4

    def pair_copy(kind, j):
        return remote(
            partials.at[slot(kind, j)], paired.at[pair_slot(j)],
            pair_send.at[j], pair_recv.at[j], partner,
        )

    def compute(kind, j):
        pair, owner, combines, _ = facts(kind, j)
        weight = pl.ds(pl.multiple_of((owner * 4 + pair * 2) * SHARD, 2 * SHARD), 2 * SHARD)

        @pl.loop(0, ROWS // TILE)
        def _(i):
            tokens = pl.ds(pl.multiple_of(i * TILE, TILE), TILE)
            part = dot(act[tokens, :], down_all[weight, :], ((1,), (1,)))
            rows = pl.ds(pl.multiple_of((kind * 4 + j) * ROWS + i * TILE, TILE), TILE)
            partials[rows, :] = part.astype(BF16)

        @pl.when(jnp.logical_not(combines))
        def _():
            pair_copy(kind, j).start()

    def add_rows(kind, j, extra, low, count):
        @pl.loop(0, count // 128)
        def _(i):
            rows = pl.ds(pl.multiple_of((kind * 4 + j) * ROWS + low + i * 128, 128), 128)
            there = pl.ds(pl.multiple_of(j * ROWS + low + i * 128, 128), 128)
            total = partials[rows, :].astype(F32) + paired[there, :].astype(F32)
            if extra is not None:
                total = total + chained[pl.ds(pl.multiple_of(extra * 512 + i * 128, 128), 128), :].astype(F32)
            partials[rows, :] = total.astype(BF16)

    def chain_copy(d, src, target):
        return remote(src, chained.at[pl.ds(d * 512, 512)], chain_send.at[d], chain_recv.at[d], target)

    def final_copy(d, src, target):
        return remote(src, final.at[pl.ds(d * ROWS, ROWS)], final_send.at[d], final_recv.at[d], target)

    def half_of(kind, j, d):
        return partials.at[pl.ds(pl.multiple_of((kind * 4 + j) * ROWS + d * 512, 512), 512)]

    def combine(kind, j):
        _, _, combines, d = facts(kind, j)

        @pl.when(combines & (d == 2))
        def _():
            pair_copy(kind, j).wait_recv()
            add_rows(kind, j, None, 0, ROWS)
            for k, by in DIRS:
                chain_copy(k, half_of(kind, j, k), y_next[by]).start()

    def relay(kind, j):
        _, _, combines, d = facts(kind, j)
        for k, by in DIRS:
            @pl.when(combines & (d == (3 if k == 0 else 1)))
            def _():
                pair_copy(kind, j).wait_recv()
                add_rows(kind, j, None, (1 - k) * 512, 512)
                chain_copy(k, half_of(kind, j, k), y_next[by]).wait_recv()
                add_rows(kind, j, k, k * 512, 512)
                final_copy(k, partials.at[slot(kind, j)], y_next[by]).start()

    down_gather.forward(0)
    compute(*BLOCKS[0])
    down_gather.third()
    combine(*BLOCKS[0])
    down_gather.forward(1)
    down_gather.forward(2)
    compute(*BLOCKS[1])
    combine(*BLOCKS[1])
    relay(*BLOCKS[0])
    compute(*BLOCKS[2])
    combine(*BLOCKS[2])
    relay(*BLOCKS[1])
    down_gather.forward(3)
    down_gather.last(0)
    compute(*BLOCKS[3])
    relay(*BLOCKS[2])
    combine(*BLOCKS[3])
    down_gather.last(1)
    down_gather.last(2)
    compute(*BLOCKS[4])
    compute(*BLOCKS[5])
    combine(*BLOCKS[4])
    relay(*BLOCKS[3])
    compute(*BLOCKS[6])
    combine(*BLOCKS[5])
    relay(*BLOCKS[4])
    down_gather.last(3)
    compute(*BLOCKS[7])
    combine(*BLOCKS[6])
    relay(*BLOCKS[5])
    combine(*BLOCKS[7])
    relay(*BLOCKS[6])
    relay(*BLOCKS[7])

    kind = jnp.where(c == own_pair, 0, 1)
    away = (y - z + 4) % 4
    j = jnp.where(away == 3, 2, jnp.where(away == 2, 3, away))
    pair_copy(kind, j).wait_recv()
    for k, by in DIRS:
        final_copy(k, partials.at[slot(kind, j)], y_next[by]).wait_recv()

    @pl.loop(0, ROWS // 128)
    def _(i):
        tokens = pl.ds(pl.multiple_of(i * 128, 128), 128)

        def rows(base):
            return pl.ds(pl.multiple_of(base * ROWS + i * 128, 128), 128)

        total = partials[rows(kind * 4 + j), :].astype(F32) + paired[rows(j), :].astype(F32)
        total = total + (final[rows(0), :].astype(F32) + final[rows(1), :].astype(F32))
        scale = inverse[tokens, :]
        scale = jnp.concatenate([scale, scale, scale], axis=1)
        out_v[tokens, :] = (stream[tokens, :].astype(F32) + scale * total).astype(BF16)

    store = pltpu.make_async_copy(out_v, result, local_sem.at[7])
    store.start()
    for copy in pending:
        copy.wait_send()
    other = 1 - kind
    for k in range(4):
        pair_copy(other, k).wait_send()
    for k, by in DIRS:
        chain_copy(k, half_of(kind, j, k), y_next[by]).wait_send()
        final_copy(k, partials.at[slot(kind, j)], y_next[by]).wait_send()
    store.wait()


def body(
    queries, key_heads, projected_value_heads, sink_logit_table, out_weight,
    residual, norm_gain, up_weight, down_weight,
):
    hbm = pl.BlockSpec(memory_space=pl.ANY)
    dma = pltpu.SemaphoreType.DMA
    return pl.pallas_call(
        kernel,
        out_shape=jax.ShapeDtypeStruct((ROWS, FEATURES), BF16),
        in_specs=[hbm, hbm, hbm, pl.BlockSpec(memory_space=pltpu.SMEM), hbm, hbm,
                  pl.BlockSpec(memory_space=pltpu.VMEM), hbm, hbm],
        out_specs=hbm,
        scratch_shapes=[
            pltpu.VMEM((D, HIDDEN), BF16),
            pltpu.VMEM((D, HIDDEN), BF16),
            pltpu.VMEM((4 * ROWS, 2 * FEATURES), BF16),
            pltpu.VMEM((8 * HEADS, ROWS), BF16),
            pltpu.VMEM((8 * HEADS, FEATURES), BF16),
            pltpu.VMEM((ROWS, HIDDEN), F32),
            pltpu.VMEM((ROWS, HIDDEN), BF16),
            pltpu.VMEM((ROWS, FEATURES), F32),
            pltpu.VMEM((ROWS, FEATURES), BF16),
            pltpu.VMEM((ROWS, FEATURES), BF16),
            pltpu.VMEM((HEADS, ROWS), BF16),
            pltpu.VMEM((HEAD_SIZE, ROWS), BF16),
            pltpu.VMEM((HEAD_SIZE, ROWS), BF16),
            pltpu.VMEM((HEAD_SIZE, WINDOW), BF16),
            pltpu.VMEM((HEAD_SIZE, WINDOW), BF16),
            pltpu.VMEM((8 * ROWS, FEATURES), BF16),
            pltpu.VMEM((4 * ROWS, FEATURES), BF16),
            pltpu.VMEM((2 * 512, FEATURES), BF16),
            pltpu.VMEM((2 * ROWS, FEATURES), BF16),
            pltpu.VMEM((64, ROWS), F32),
            pltpu.VMEM((ROWS, 128), F32),
            pltpu.VMEM((ROWS, FEATURES), BF16),
            dma((8,)), dma((7,)), dma((7,)), dma((2,)), dma((2,)), dma((80,)), dma((80,)),
            dma((8,)), dma((8,)), dma((10,)), dma((10,)), dma((7,)), dma((7,)),
            dma((4,)), dma((4,)), dma((2,)), dma((2,)), dma((2,)), dma((2,)),
        ],
        compiler_params=pltpu.CompilerParams(
            collective_id=0, has_side_effects=True, vmem_limit_bytes=67043328
        ),
    )(
        queries.T, key_heads.T, projected_value_heads.T, sink_logit_table, out_weight,
        residual, norm_gain.reshape(1, FEATURES), up_weight, down_weight.T,
    )


def solution(mesh):
    return jax.shard_map(
        body,
        mesh=mesh,
        in_specs=(
            P("sp", "tp"), P("sp", "tp"), P("sp", "tp"), P("tp"), P("tp", None),
            P("sp", "tp"), P("tp"), P("sp", "tp"), P("tp", "sp"),
        ),
        out_specs=P("sp", "tp"),
        check_vma=False,
    )
```

time: 257 us -> 167 us (0.65)
  the two profiles are of different devices: /device:TPU:9 before, /device:TPU:22 now
where the time goes in v1:
time: 167 us
  Pallas kernels  163 us (98%)
  local copies, waits for them, and re-layouts  3.33 us (2%)
    pallas_call x1, Pallas kernels, body(): pl.pallas_call(kernel, out_shape=jax.ShapeDtypeStruct((ROWS, FEATURES), B...  163 us

profile of v1, /device:TPU:22, one launch (start us, length us, event | category | flops | bytes accessed | tf_op | source)
XLA Modules:
  0.0 166.5 jit_solution(3051166134022205165)
XLA Ops:
  0.0 1.2 reshape.3.gain
  1.2 163.2 %shard_map.91 = bf16[1024,384]{1,0:T(8,128)(2,1)} custom-call(bf16[192,1024]{1,0:T(8,128)(2,1)} %bitcast.5, bf16[64,1024]{1,0:T(8,128)(2,1)} %bitcast.6, bf16[64,1024]{1,0:T(8,128)(2,1)} %bitcast.7, f32[3]{0:T(128)} %sink.1, bf16[192,3072]{1,0:T(8,128)(2,1)} %out_weight.1, bf16[1024,384]{1,0:T(8,128)(2,1)} %residual.1, bf16[1,384]{1,0:T(2,128)(2,1)} %reshape.3.gain, ...), custom_call_target="tpu_custom_call" | custom-call | tf_op jit(solution)/shard_map/pallas_call | solution.py:516
  164.5 2.1 %copy.11 = bf16[1024,384]{1,0:T(8,128)(2,1)} copy(bf16[1024,384]{1,0:T(8,128)(2,1)} %shard_map.91) | data formatting | bytes 1572864

commit v2 on v1

--- a/solution.py
+++ b/solution.py
@@ -33,11 +33,11 @@
 def kernel(
     queries, keys, values, sink, out_weight, residual, gain, up, down,
     result,
-    up_all, down_all, x_all, att_all, w_all, hidden, act, mixed, stream, res_v,
-    q_v, k_v, v_v, halo_k, halo_v, partials, paired, chained, final, squares, inverse, out_v,
+    up_all, down_all, x_all, att_all, w_all, w_pass, hidden, act_t, mixed, stream, res_v,
+    q_v, k_v, v_v, halo_k, halo_v, partials, paired, chained, final, squares, out_v,
     local_sem, w_send, w_recv, halo_send, halo_recv, g_send, g_recv,
     att_send, att_recv, x_send, x_recv, sq_send, sq_recv,
-    pair_send, pair_recv, chain_send, chain_recv, final_send, final_recv,
+    pair_send, pair_recv, chain_send, chain_recv,
 ):
     s, t = lax.axis_index("sp"), lax.axis_index("tp")
     z, x = s // 4, s % 4
@@ -171,8 +171,6 @@
 
     up_gather = Gather(up, up_all, 0)
     down_gather = Gather(down, down_all, 40)
-    up_gather.first()
-
     after = ((s + 1) % 16, t)
     tail = pl.ds(ROWS - WINDOW, WINDOW)
     halo_copies = [
@@ -181,16 +179,39 @@
     ]
     for copy in halo_copies:
         start(copy)
-    w_mine = w_all.at[pl.ds(pl.multiple_of(t * HEADS, HEADS), HEADS)]
-    w_copies = []
-    for k in range(1, 8):
-        owner = (t + k) % 8
-        copy = remote(
-            out_weight.at[:, pl.ds(pl.multiple_of(owner * FEATURES, 128), FEATURES)],
-            w_mine, w_send.at[k - 1], w_recv.at[k - 1], (s, owner),
-        )
-        start(copy)
-        w_copies.append(copy)
+    up_gather.first()
+
+    def w_cols(yy, cc=0, count=FEATURES):
+        return pl.ds(pl.multiple_of((yy * 2 + cc) * FEATURES, 128), count)
+
+    def w_rows(yy, cc, low=0, count=HEADS):
+        return w_all.at[pl.ds(pl.multiple_of((yy * 2 + cc) * HEADS + low, 32), count)]
+
+    def w_relay(k, by):
+        src = out_weight.at[pl.ds(k * HALF, HALF), w_cols(ring(y, 2), 0, 2 * FEATURES)]
+        return remote(src, w_pass.at[k], w_send.at[5 + k], w_recv.at[5 + k], y_next[by])
+
+    for k, by in DIRS:
+        start(w_relay(k, by))
+    start(remote(out_weight.at[:, w_cols(y, 1 - c)], w_rows(y, c), w_send.at[0], w_recv.at[0], partner))
+    for k, by in DIRS:
+        for cc in (0, 1):
+            start(remote(
+                out_weight.at[:, w_cols(ring(y, by), cc)], w_rows(y, c),
+                w_send.at[1 + 2 * k + cc], w_recv.at[1 + 2 * k + c], (s, ring(y, by) * 2 + cc),
+            ))
+
+    def w_arrived(index, ref):
+        remote(ref, ref, w_send.at[index], w_recv.at[index], partner).wait_recv()
+
+    def w_pass_on():
+        for k, by in DIRS:
+            w_relay(k, by).wait_recv()
+            for cc in (0, 1):
+                start(remote(
+                    w_pass.at[k, :, pl.ds(cc * FEATURES, FEATURES)], w_rows(ring(y, -by), c, k * HALF, HALF),
+                    w_send.at[7 + 2 * k + cc], w_recv.at[7 + 2 * k + c], (s, ring(y, by) * 2 + cc),
+                ))
 
     sinks = jnp.concatenate([jnp.full((1, WINDOW), sink[g], F32) for g in range(3)], axis=1)
     key_at = lax.broadcasted_iota(jnp.int32, (2 * WINDOW, 3 * WINDOW), 0)
@@ -243,12 +264,11 @@
     for d, by in DIRS:
         start(att_copy(d, att_rows(y, c), y_next[by]))
     start(att_copy(4, att_rows(y, c), partner))
+    w_pass_on()
     up_gather.second()
 
     for i, copy in enumerate(locals_[3:]):
         copy.wait()
-    for copy in w_copies:
-        copy.wait_recv()
 
     def mix(yy, first):
         rows = pl.ds(pl.multiple_of(yy * 2 * HEADS, 2 * HEADS), 2 * HEADS)
@@ -260,19 +280,27 @@
             mixed[tokens, :] = part if first else mixed[tokens, :] + part
 
     att_arrived(4, att_rows(y, 1 - c))
+    w_arrived(0, w_rows(y, 1 - c))
     mix(y, True)
+    up_gather.forward(0)
+    up_gather.third()
     for d, by in DIRS:
         att_arrived(d, att_rows(ring(y, -by), c))
         start(att_copy(2 + d, att_rows(ring(y, -by), c, d * HALF, HALF), y_next[by]))
         start(att_copy(5 + d, att_rows(ring(y, -by), c), partner))
-    up_gather.third()
     for d, by in DIRS:
         att_arrived(5 + d, att_rows(ring(y, -by), 1 - c))
+        for cc in (0, 1):
+            w_arrived(1 + 2 * d + cc, w_rows(ring(y, -by), cc))
         mix(ring(y, -by), False)
+    up_gather.forward(1)
     for d, by in DIRS:
         att_arrived(2 + d, att_rows(ring(y, 2), c, d * HALF, HALF))
     start(att_copy(7, att_rows(ring(y, 2), c), partner))
     att_arrived(7, att_rows(ring(y, 2), 1 - c))
+    for d, by in DIRS:
+        for cc in (0, 1):
+            w_arrived(7 + 2 * d + cc, w_rows(ring(y, 2), cc, d * HALF, HALF))
     mix(ring(y, 2), False)
 
     lanes_of = lambda cc: pl.ds(pl.multiple_of(cc * FEATURES, 128), FEATURES)
@@ -280,7 +308,7 @@
     def x_block(yy, cc, low=0, count=ROWS):
         return x_all.at[pl.ds(pl.multiple_of(yy * ROWS + low, 512), count), lanes_of(cc)]
 
-    gains = gain[...].astype(F32)
+    gains = gain[...].astype(F32).reshape(1, FEATURES)
     ones = jnp.ones((8, FEATURES), BF16)
     sq_rows = pl.ds(pl.multiple_of(t * 8, 8), 8)
 
@@ -313,14 +341,12 @@
         start(copy)
         sq_copies.append(copy)
 
-    up_gather.forward(0)
-    up_gather.forward(1)
     up_gather.forward(2)
+    up_gather.forward(3)
+    down_gather.first()
     x_arrived(0, x_block(ring(y, -1), c, 0, 512))
     start(x_copy(4, x_block(ring(y, -1), c, 0, 512), y_next[1]))
     x_arrived(1, x_block(ring(y, 1), c, 0, 512))
-    up_gather.forward(3)
-    down_gather.first()
     x_arrived(3, x_block(ring(y, 1), c, 512, 512))
     start(x_copy(5, x_block(ring(y, 1), c, 512, 512), y_next[-1]))
     x_arrived(2, x_block(ring(y, -1), c, 512, 512))
@@ -338,7 +364,8 @@
                 if not first:
                     part = part + hidden[tokens, cols]
                 if last:
-                    act[tokens, cols] = jnp.square(jnp.maximum(part, 0.0)).astype(BF16)
+                    units = jnp.square(jnp.maximum(part, 0.0)).astype(BF16)
+                    act_t[cols, tokens] = jnp.transpose(units)
                 else:
                     hidden[tokens, cols] = part
 
@@ -349,161 +376,195 @@
     for d, by in DIRS:
         x_arrived(7 + d, x_block(ring(y, -by), 1 - c))
         hide(ring(y, -by), False, False)
+        if d == 0:
+            down_gather.second()
     x_arrived(4, x_block(ring(y, 2), c, 0, 512))
     x_arrived(5, x_block(ring(y, 2), c, 512, 512))
     start(x_copy(9, x_block(ring(y, 2), c), partner))
-    down_gather.second()
     x_arrived(9, x_block(ring(y, 2), 1 - c))
     hide(ring(y, 2), False, True)
 
-    for copy in sq_copies:
-        copy.wait_recv()
-    total = jnp.zeros((1, ROWS), F32)
-    for k in range(8):
-        total = total + squares[pl.ds(8 * k, 1), :]
-    factor = 1.0 / (total * (1.0 / D) + EPSILON)
-    inverse[...] = jnp.transpose(jnp.broadcast_to(factor, (128, ROWS)))
-
-    own_pair = x // 2
-    BLOCKS = ((0, 0), (0, 1), (0, 2), (1, 0), (0, 3), (1, 1), (1, 2), (1, 3))
-    SHIFT = (0, 1, -1, 2)
-
-    def slot(kind, j):
-        return pl.ds(pl.multiple_of((kind * 4 + j) * ROWS, ROWS), ROWS)
-
-    def pair_slot(j):
-        return pl.ds(pl.multiple_of(j * ROWS, ROWS), ROWS)
-
-    def facts(kind, j):
-        pair = own_pair if kind == 0 else 1 - own_pair
-        owner = ring(z, SHIFT[j])
-        return pair, owner, c == pair, (y - owner + 4) % 4
-
-    def pair_copy(kind, j):
-        return remote(
-            partials.at[slot(kind, j)], paired.at[pair_slot(j)],
-            pair_send.at[j], pair_recv.at[j], partner,
-        )
-
-    def compute(kind, j):
-        pair, owner, combines, _ = facts(kind, j)
-        weight = pl.ds(pl.multiple_of((owner * 4 + pair * 2) * SHARD, 2 * SHARD), 2 * SHARD)
-
+    GROUPS = (
+        [(0, 0, j) for j in range(4)],
+        [(1, 0, j) for j in range(4)],
+        [(0, i, j) for j in (0, 1) for i in (1, 2)],
+        [(1, i, j) for j in (0, 1) for i in (1, 2)],
+        [(0, i, j) for j in (2, 3) for i in (1, 2)],
+        [(1, i, j) for j in (2, 3) for i in (1, 2)],
+        [(half, 3, j) for half in (0, 1) for j in (0, 1)],
+        [(half, 3, j) for half in (0, 1) for j in (2, 3)],
+    )
+
+    class Piece:
+        def __init__(self, half, i, j):
+            sec, prim = down_gather.at(half)
+            sec, prim = ring(sec, STEPS[i]), ring(prim, STEPS[j])
+            zz, xx = (sec, prim) if half == 0 else (prim, sec)
+            self.row = (zz * 4 + xx) * SHARD + half * HALF
+            self.part = (xx % 2) * 2 + half
+            self.mine = xx // 2 == c
+            self.away = (y - zz + 4) % 4
+            self.pair = zz * 4 + self.part
+
+        def rows(self, low=0, count=HALF):
+            return pl.ds(pl.multiple_of(self.row + low, 16), count)
+
+        def paired_rows(self, low=0, count=HALF):
+            return pl.ds(pl.multiple_of(self.pair * HALF + low, 16), count)
+
+        def to_pair(self):
+            return remote(
+                partials.at[self.rows()], paired.at[self.paired_rows()],
+                pair_send.at[self.pair], pair_recv.at[self.pair], partner,
+            )
+
+        def hop(self, step, k, by):
+            index = step * 8 + k * 4 + self.part
+            if step < 2:
+                dst = chained.at[pl.ds(pl.multiple_of(index * QUARTER, 16), QUARTER)]
+            else:
+                dst = final.at[pl.ds(pl.multiple_of(self.part * HALF + k * QUARTER, 16), QUARTER)]
+            return remote(
+                partials.at[self.rows(k * QUARTER, QUARTER)], dst,
+                chain_send.at[index], chain_recv.at[index], y_next[by],
+            )
+
+        def add_pair(self, k):
+            rows = self.rows(k * QUARTER, QUARTER)
+            total = partials[rows, :].astype(F32) + paired[self.paired_rows(k * QUARTER, QUARTER), :].astype(F32)
+            partials[rows, :] = total.astype(BF16)
+
+        def add_hop(self, step, k):
+            rows = self.rows(k * QUARTER, QUARTER)
+            there = pl.ds(pl.multiple_of((step * 8 + k * 4 + self.part) * QUARTER, 16), QUARTER)
+            total = partials[rows, :].astype(F32) + chained[there, :].astype(F32)
+            partials[rows, :] = total.astype(BF16)
+
+    groups = [[Piece(*facts) for facts in group] for group in GROUPS]
+
+    def compute(group):
         @pl.loop(0, ROWS // TILE)
         def _(i):
             tokens = pl.ds(pl.multiple_of(i * TILE, TILE), TILE)
-            part = dot(act[tokens, :], down_all[weight, :], ((1,), (1,)))
-            rows = pl.ds(pl.multiple_of((kind * 4 + j) * ROWS + i * TILE, TILE), TILE)
-            partials[rows, :] = part.astype(BF16)
-
-        @pl.when(jnp.logical_not(combines))
-        def _():
-            pair_copy(kind, j).start()
-
-    def add_rows(kind, j, extra, low, count):
-        @pl.loop(0, count // 128)
-        def _(i):
-            rows = pl.ds(pl.multiple_of((kind * 4 + j) * ROWS + low + i * 128, 128), 128)
-            there = pl.ds(pl.multiple_of(j * ROWS + low + i * 128, 128), 128)
-            total = partials[rows, :].astype(F32) + paired[there, :].astype(F32)
-            if extra is not None:
-                total = total + chained[pl.ds(pl.multiple_of(extra * 512 + i * 128, 128), 128), :].astype(F32)
-            partials[rows, :] = total.astype(BF16)
-
-    def chain_copy(d, src, target):
-        return remote(src, chained.at[pl.ds(d * 512, 512)], chain_send.at[d], chain_recv.at[d], target)
-
-    def final_copy(d, src, target):
-        return remote(src, final.at[pl.ds(d * ROWS, ROWS)], final_send.at[d], final_recv.at[d], target)
-
-    def half_of(kind, j, d):
-        return partials.at[pl.ds(pl.multiple_of((kind * 4 + j) * ROWS + d * 512, 512), 512)]
-
-    def combine(kind, j):
-        _, _, combines, d = facts(kind, j)
-
-        @pl.when(combines & (d == 2))
-        def _():
-            pair_copy(kind, j).wait_recv()
-            add_rows(kind, j, None, 0, ROWS)
+            weight = jnp.concatenate([down_all[p.rows(), :] for p in group], axis=0)
+            part = dot(weight, act_t[:, tokens], ((1,), (0,))).astype(BF16)
+            for k, p in enumerate(group):
+                partials[p.rows(), tokens] = part[k * HALF : (k + 1) * HALF]
+
+        for p in group:
+            @pl.when(jnp.logical_not(p.mine))
+            def _():
+                p.to_pair().start()
+
+    def combine(group):
+        for p in group:
+            @pl.when(p.mine & (p.away != 0))
+            def _():
+                p.to_pair().wait_recv()
+                for k in (0, 1):
+                    p.add_pair(k)
+                for k, by in DIRS:
+                    @pl.when(p.away == (1 if k == 0 else 3))
+                    def _():
+                        p.hop(0, k, by).start()
+
+    def relay(group):
+        for p in group:
+            @pl.when(p.mine & (p.away == 2))
+            def _():
+                for k, by in DIRS:
+                    p.hop(0, k, by).wait_recv()
+                    p.add_hop(0, k)
+                    p.hop(1, k, by).start()
+
+    def deliver(group):
+        for p in group:
             for k, by in DIRS:
-                chain_copy(k, half_of(kind, j, k), y_next[by]).start()
-
-    def relay(kind, j):
-        _, _, combines, d = facts(kind, j)
+                @pl.when(p.mine & (p.away == (3 if k == 0 else 1)))
+                def _():
+                    p.hop(1, k, by).wait_recv()
+                    p.add_hop(1, k)
+                    p.hop(2, k, by).start()
+
+    down_gather.forward(0)
+    down_gather.third()
+    compute(groups[0])
+    compute(groups[1])
+    combine(groups[0])
+    combine(groups[1])
+    down_gather.forward(1)
+    compute(groups[2])
+    relay(groups[0])
+    compute(groups[3])
+    relay(groups[1])
+    combine(groups[2])
+    combine(groups[3])
+    deliver(groups[0])
+    deliver(groups[1])
+    down_gather.forward(2)
+    relay(groups[2])
+    relay(groups[3])
+    down_gather.forward(3)
+    compute(groups[4])
+    deliver(groups[2])
+    compute(groups[5])
+    combine(groups[4])
+    combine(groups[5])
+    deliver(groups[3])
+    down_gather.last(0)
+    down_gather.last(1)
+    compute(groups[6])
+    relay(groups[4])
+    relay(groups[5])
+    combine(groups[6])
+    deliver(groups[4])
+    deliver(groups[5])
+    down_gather.last(2)
+    down_gather.last(3)
+    compute(groups[7])
+    relay(groups[6])
+    combine(groups[7])
+    deliver(groups[6])
+    relay(groups[7])
+    deliver(groups[7])
+
+    for copy in sq_copies:
+        copy.wait_recv()
+    own = [Piece(half, 0, 0) for half in (0, 1, 0, 1)]
+    for part, p in enumerate(own):
+        p.part = part
+        p.row = (y * 4 + c * 2) * SHARD + part * HALF
+        p.pair = y * 4 + part
+    for p in own:
+        p.to_pair().wait_recv()
         for k, by in DIRS:
-            @pl.when(combines & (d == (3 if k == 0 else 1)))
-            def _():
-                pair_copy(kind, j).wait_recv()
-                add_rows(kind, j, None, (1 - k) * 512, 512)
-                chain_copy(k, half_of(kind, j, k), y_next[by]).wait_recv()
-                add_rows(kind, j, k, k * 512, 512)
-                final_copy(k, partials.at[slot(kind, j)], y_next[by]).start()
-
-    down_gather.forward(0)
-    compute(*BLOCKS[0])
-    down_gather.third()
-    combine(*BLOCKS[0])
-    down_gather.forward(1)
-    down_gather.forward(2)
-    compute(*BLOCKS[1])
-    combine(*BLOCKS[1])
-    relay(*BLOCKS[0])
-    compute(*BLOCKS[2])
-    combine(*BLOCKS[2])
-    relay(*BLOCKS[1])
-    down_gather.forward(3)
-    down_gather.last(0)
-    compute(*BLOCKS[3])
-    relay(*BLOCKS[2])
-    combine(*BLOCKS[3])
-    down_gather.last(1)
-    down_gather.last(2)
-    compute(*BLOCKS[4])
-    compute(*BLOCKS[5])
-    combine(*BLOCKS[4])
-    relay(*BLOCKS[3])
-    compute(*BLOCKS[6])
-    combine(*BLOCKS[5])
-    relay(*BLOCKS[4])
-    down_gather.last(3)
-    compute(*BLOCKS[7])
-    combine(*BLOCKS[6])
-    relay(*BLOCKS[5])
-    combine(*BLOCKS[7])
-    relay(*BLOCKS[6])
-    relay(*BLOCKS[7])
-
-    kind = jnp.where(c == own_pair, 0, 1)
-    away = (y - z + 4) % 4
-    j = jnp.where(away == 3, 2, jnp.where(away == 2, 3, away))
-    pair_copy(kind, j).wait_recv()
-    for k, by in DIRS:
-        final_copy(k, partials.at[slot(kind, j)], y_next[by]).wait_recv()
+            p.hop(2, k, by).wait_recv()
+    mine = pl.ds(pl.multiple_of((y * 4 + c * 2) * SHARD, FEATURES), FEATURES)
+    beside = pl.ds(pl.multiple_of(y * FEATURES, FEATURES), FEATURES)
 
     @pl.loop(0, ROWS // 128)
     def _(i):
         tokens = pl.ds(pl.multiple_of(i * 128, 128), 128)
-
-        def rows(base):
-            return pl.ds(pl.multiple_of(base * ROWS + i * 128, 128), 128)
-
-        total = partials[rows(kind * 4 + j), :].astype(F32) + paired[rows(j), :].astype(F32)
-        total = total + (final[rows(0), :].astype(F32) + final[rows(1), :].astype(F32))
-        scale = inverse[tokens, :]
-        scale = jnp.concatenate([scale, scale, scale], axis=1)
-        out_v[tokens, :] = (stream[tokens, :].astype(F32) + scale * total).astype(BF16)
+        total = partials[mine, tokens].astype(F32) + paired[beside, tokens].astype(F32)
+        total = total + final[:, tokens].astype(F32)
+        norm = squares[0:1, tokens]
+        for k in range(1, 8):
+            norm = norm + squares[8 * k : 8 * k + 1, tokens]
+        total = total * (1.0 / (norm * (1.0 / D) + EPSILON))
+        out_v[tokens, :] = (stream[tokens, :].astype(F32) + jnp.transpose(total)).astype(BF16)
 
     store = pltpu.make_async_copy(out_v, result, local_sem.at[7])
     store.start()
     for copy in pending:
         copy.wait_send()
-    other = 1 - kind
-    for k in range(4):
-        pair_copy(other, k).wait_send()
-    for k, by in DIRS:
-        chain_copy(k, half_of(kind, j, k), y_next[by]).wait_send()
-        final_copy(k, partials.at[slot(kind, j)], y_next[by]).wait_send()
+    for k in range(16):
+        p = own[0]
+        p.pair = k
+        p.to_pair().wait_send()
+    for p in own:
+        for k, by in DIRS:
+            for step in range(3):
+                p.hop(step, k, by).wait_send()
     store.wait()
 
 
@@ -525,8 +586,9 @@
             pltpu.VMEM((4 * ROWS, 2 * FEATURES), BF16),
             pltpu.VMEM((8 * HEADS, ROWS), BF16),
             pltpu.VMEM((8 * HEADS, FEATURES), BF16),
+            pltpu.VMEM((2, HALF, 2 * FEATURES), BF16),
             pltpu.VMEM((ROWS, HIDDEN), F32),
-            pltpu.VMEM((ROWS, HIDDEN), BF16),
+            pltpu.VMEM((HIDDEN, ROWS), BF16),
             pltpu.VMEM((ROWS, FEATURES), F32),
             pltpu.VMEM((ROWS, FEATURES), BF16),
             pltpu.VMEM((ROWS, FEATURES), BF16),
@@ -535,23 +597,22 @@
             pltpu.VMEM((HEAD_SIZE, ROWS), BF16),
             pltpu.VMEM((HEAD_SIZE, WINDOW), BF16),
             pltpu.VMEM((HEAD_SIZE, WINDOW), BF16),
-            pltpu.VMEM((8 * ROWS, FEATURES), BF16),
-            pltpu.VMEM((4 * ROWS, FEATURES), BF16),
-            pltpu.VMEM((2 * 512, FEATURES), BF16),
-            pltpu.VMEM((2 * ROWS, FEATURES), BF16),
+            pltpu.VMEM((D, ROWS), BF16),
+            pltpu.VMEM((D // 2, ROWS), BF16),
+            pltpu.VMEM((16 * QUARTER, ROWS), BF16),
+            pltpu.VMEM((FEATURES, ROWS), BF16),
             pltpu.VMEM((64, ROWS), F32),
-            pltpu.VMEM((ROWS, 128), F32),
             pltpu.VMEM((ROWS, FEATURES), BF16),
-            dma((8,)), dma((7,)), dma((7,)), dma((2,)), dma((2,)), dma((80,)), dma((80,)),
+            dma((8,)), dma((11,)), dma((11,)), dma((2,)), dma((2,)), dma((80,)), dma((80,)),
             dma((8,)), dma((8,)), dma((10,)), dma((10,)), dma((7,)), dma((7,)),
-            dma((4,)), dma((4,)), dma((2,)), dma((2,)), dma((2,)), dma((2,)),
+            dma((16,)), dma((16,)), dma((24,)), dma((24,)),
         ],
         compiler_params=pltpu.CompilerParams(
             collective_id=0, has_side_effects=True, vmem_limit_bytes=67043328
         ),
     )(
         queries.T, key_heads.T, projected_value_heads.T, sink_logit_table, out_weight,
-        residual, norm_gain.reshape(1, FEATURES), up_weight, down_weight.T,
+        residual, norm_gain, up_weight, down_weight.T,
     )
 
 

time: 167 us -> 135 us (0.81)
  the two profiles are of different devices: /device:TPU:22 before, /device:TPU:9 now
where the time goes in v2:
time: 135 us; the launch traced here: 134 us
  Pallas kernels  132 us (98%)
  local copies, waits for them, and re-layouts  2.09 us (2%)
    pallas_call x1, Pallas kernels, body(): pl.pallas_call(kernel, out_shape=jax.ShapeDtypeStruct((ROWS, FEATURES), B...  132 us

profile of v2, /device:TPU:9, one launch (start us, length us, event | category | flops | bytes accessed | tf_op | source)
XLA Modules:
  0.0 134.0 jit_solution(11646562294728015324)
XLA Ops:
  0.0 131.9 %shard_map.91 = bf16[1024,384]{1,0:T(8,128)(2,1)} custom-call(bf16[192,1024]{1,0:T(8,128)(2,1)} %bitcast.5, bf16[64,1024]{1,0:T(8,128)(2,1)} %bitcast.6, bf16[64,1024]{1,0:T(8,128)(2,1)} %bitcast.7, f32[3]{0:T(128)} %sink.1, bf16[192,3072]{1,0:T(8,128)(2,1)} %out_weight.1, bf16[1024,384]{1,0:T(8,128)(2,1)} %residual.1, bf16[384]{0:T(512)(128)(2,1)} %gain.1, ...), custom_call_target="tpu_custom_call" | custom-call | tf_op jit(solution)/shard_map/pallas_call | solution.py:577
  131.9 2.1 %copy.11 = bf16[1024,384]{1,0:T(8,128)(2,1)} copy(bf16[1024,384]{1,0:T(8,128)(2,1)} %shard_map.91) | data formatting | bytes 1572864

commit v3 on v2

--- a/solution.py
+++ b/solution.py
@@ -31,13 +31,13 @@
 
 
 def kernel(
-    queries, keys, values, sink, out_weight, residual, gain, up, down,
+    queries, keys, values, sinks_in, out_weight, residual, gains_in, up, down,
     result,
     up_all, down_all, x_all, att_all, w_all, w_pass, hidden, act_t, mixed, stream, res_v,
-    q_v, k_v, v_v, halo_k, halo_v, partials, paired, chained, final, squares, out_v,
+    q_v, k_v, v_v, halo_k, halo_v, partials, paired, final, squares, sink, gain,
     local_sem, w_send, w_recv, halo_send, halo_recv, g_send, g_recv,
     att_send, att_recv, x_send, x_recv, sq_send, sq_recv,
-    pair_send, pair_recv, chain_send, chain_recv,
+    pair_send, pair_recv, owner_send, owner_recv,
 ):
     s, t = lax.axis_index("sp"), lax.axis_index("tp")
     z, x = s // 4, s % 4
@@ -76,7 +76,7 @@
     locals_ = [
         pltpu.make_async_copy(src, dst, local_sem.at[i])
         for i, (src, dst) in enumerate([
-            (queries, q_v), (keys, k_v), (values, v_v), (residual, res_v),
+            (queries, q_v), (keys, k_v), (values, v_v), (sinks_in, sink), (gains_in, gain), (residual, res_v),
             (up, up_all.at[pl.ds(pl.multiple_of(s * SHARD, SHARD), SHARD)]),
             (down, down_all.at[pl.ds(pl.multiple_of(s * SHARD, SHARD), SHARD)]),
             (out_weight.at[:, pl.ds(pl.multiple_of(t * FEATURES, 128), FEATURES)],
@@ -88,6 +88,7 @@
     pl.semaphore_wait(barrier, len(greeted))
 
     STEPS = (0, -1, 1, 2)
+    ORDER = ((0, 1, 2, 3), (0, 1, 3, 2))
 
     class Gather:
         def __init__(self, own, buf, base):
@@ -137,8 +138,7 @@
                     piece = self.spot(half, sec, origin, d * QUARTER, QUARTER)
                     start(self.copy(half, 2 + d, piece, piece, self.towards(half, True, by)))
             for half in (0, 1):
-                for j in (1, 2):
-                    self.spread(half, j)
+                self.spread(half, 1)
 
         def spread(self, half, j):
             sec, prim = self.at(half)
@@ -146,15 +146,23 @@
             for d, by in DIRS:
                 start(self.copy(half, 4 + 2 * j + d, piece, piece, self.towards(half, False, by)))
 
+        def opposite(self, half):
+            sec, prim = self.at(half)
+            for d, by in DIRS:
+                self.wait(half, 2 + d, sec, ring(prim, 2), d * QUARTER, QUARTER)
+            self.spread(half, 3)
+
         def third(self):
+            self.spread(0, 2)
+            self.opposite(1)
+
+        def fourth(self):
+            self.spread(1, 2)
+            self.opposite(0)
+
+        def forward(self, k):
             for half in (0, 1):
-                sec, prim = self.at(half)
-                for d, by in DIRS:
-                    self.wait(half, 2 + d, sec, ring(prim, 2), d * QUARTER, QUARTER)
-                self.spread(half, 3)
-
-        def forward(self, j):
-            for half in (0, 1):
+                j = ORDER[half][k]
                 sec, prim = self.at(half)
                 origin = ring(prim, STEPS[j])
                 for d, by in DIRS:
@@ -162,8 +170,9 @@
                     piece = self.spot(half, ring(sec, -by), origin, d * QUARTER, QUARTER)
                     start(self.copy(half, 12 + 2 * j + d, piece, piece, self.towards(half, False, by)))
 
-        def last(self, j):
+        def last(self, k):
             for half in (0, 1):
+                j = ORDER[half][k]
                 sec, prim = self.at(half)
                 origin = ring(prim, STEPS[j])
                 for d, by in DIRS:
@@ -213,7 +222,6 @@
                     w_send.at[7 + 2 * k + cc], w_recv.at[7 + 2 * k + c], (s, ring(y, by) * 2 + cc),
                 ))
 
-    sinks = jnp.concatenate([jnp.full((1, WINDOW), sink[g], F32) for g in range(3)], axis=1)
     key_at = lax.broadcasted_iota(jnp.int32, (2 * WINDOW, 3 * WINDOW), 0)
     query_at = lax.broadcasted_iota(jnp.int32, (2 * WINDOW, 3 * WINDOW), 1) % WINDOW
     mine_row = t * HEADS
@@ -233,8 +241,9 @@
             att_all[rows, lanes] = output[:, g * WINDOW : (g + 1) * WINDOW]
 
     near = (key_at > query_at) & (key_at <= query_at + WINDOW)
-    for copy in locals_[:3]:
+    for copy in locals_[:4]:
         copy.wait()
+    sinks = jnp.concatenate([jnp.full((1, WINDOW), sink[g], F32) for g in range(3)], axis=1)
 
     @pl.loop(1, 8)
     def _(n):
@@ -267,7 +276,7 @@
     w_pass_on()
     up_gather.second()
 
-    for i, copy in enumerate(locals_[3:]):
+    for copy in locals_[4:]:
         copy.wait()
 
     def mix(yy, first):
@@ -294,6 +303,7 @@
             w_arrived(1 + 2 * d + cc, w_rows(ring(y, -by), cc))
         mix(ring(y, -by), False)
     up_gather.forward(1)
+    up_gather.fourth()
     for d, by in DIRS:
         att_arrived(2 + d, att_rows(ring(y, 2), c, d * HALF, HALF))
     start(att_copy(7, att_rows(ring(y, 2), c), partner))
@@ -342,11 +352,11 @@
         sq_copies.append(copy)
 
     up_gather.forward(2)
-    up_gather.forward(3)
-    down_gather.first()
     x_arrived(0, x_block(ring(y, -1), c, 0, 512))
     start(x_copy(4, x_block(ring(y, -1), c, 0, 512), y_next[1]))
     x_arrived(1, x_block(ring(y, 1), c, 0, 512))
+    up_gather.forward(3)
+    down_gather.first()
     x_arrived(3, x_block(ring(y, 1), c, 512, 512))
     start(x_copy(5, x_block(ring(y, 1), c, 512, 512), y_next[-1]))
     x_arrived(2, x_block(ring(y, -1), c, 512, 512))
@@ -384,16 +394,10 @@
     x_arrived(9, x_block(ring(y, 2), 1 - c))
     hide(ring(y, 2), False, True)
 
-    GROUPS = (
-        [(0, 0, j) for j in range(4)],
-        [(1, 0, j) for j in range(4)],
-        [(0, i, j) for j in (0, 1) for i in (1, 2)],
-        [(1, i, j) for j in (0, 1) for i in (1, 2)],
-        [(0, i, j) for j in (2, 3) for i in (1, 2)],
-        [(1, i, j) for j in (2, 3) for i in (1, 2)],
-        [(half, 3, j) for half in (0, 1) for j in (0, 1)],
-        [(half, 3, j) for half in (0, 1) for j in (2, 3)],
-    )
+    GROUPS = [[(half, 0, j) for j in range(4)] for half in (0, 1)]
+    for k in range(4):
+        GROUPS.append([(half, i, ORDER[half][k]) for half in (0, 1) for i in (1, 2)])
+        GROUPS.append([(half, 3, ORDER[half][k]) for half in (0, 1)])
 
     class Piece:
         def __init__(self, half, i, j):
@@ -418,26 +422,16 @@
                 pair_send.at[self.pair], pair_recv.at[self.pair], partner,
             )
 
-        def hop(self, step, k, by):
-            index = step * 8 + k * 4 + self.part
-            if step < 2:
-                dst = chained.at[pl.ds(pl.multiple_of(index * QUARTER, 16), QUARTER)]
-            else:
-                dst = final.at[pl.ds(pl.multiple_of(self.part * HALF + k * QUARTER, 16), QUARTER)]
+        def to_owner(self):
+            index = (self.away - 1) * 4 + self.part
             return remote(
-                partials.at[self.rows(k * QUARTER, QUARTER)], dst,
-                chain_send.at[index], chain_recv.at[index], y_next[by],
+                partials.at[self.rows()], final.at[pl.ds(pl.multiple_of(index * HALF, 32), HALF)],
+                owner_send.at[index], owner_recv.at[index], (s, ring(y, -self.away) * 2 + c),
             )
 
         def add_pair(self, k):
             rows = self.rows(k * QUARTER, QUARTER)
             total = partials[rows, :].astype(F32) + paired[self.paired_rows(k * QUARTER, QUARTER), :].astype(F32)
-            partials[rows, :] = total.astype(BF16)
-
-        def add_hop(self, step, k):
-            rows = self.rows(k * QUARTER, QUARTER)
-            there = pl.ds(pl.multiple_of((step * 8 + k * 4 + self.part) * QUARTER, 16), QUARTER)
-            total = partials[rows, :].astype(F32) + chained[there, :].astype(F32)
             partials[rows, :] = total.astype(BF16)
 
     groups = [[Piece(*facts) for facts in group] for group in GROUPS]
@@ -463,70 +457,38 @@
                 p.to_pair().wait_recv()
                 for k in (0, 1):
                     p.add_pair(k)
-                for k, by in DIRS:
-                    @pl.when(p.away == (1 if k == 0 else 3))
-                    def _():
-                        p.hop(0, k, by).start()
-
-    def relay(group):
-        for p in group:
-            @pl.when(p.mine & (p.away == 2))
-            def _():
-                for k, by in DIRS:
-                    p.hop(0, k, by).wait_recv()
-                    p.add_hop(0, k)
-                    p.hop(1, k, by).start()
-
-    def deliver(group):
-        for p in group:
-            for k, by in DIRS:
-                @pl.when(p.mine & (p.away == (3 if k == 0 else 1)))
-                def _():
-                    p.hop(1, k, by).wait_recv()
-                    p.add_hop(1, k)
-                    p.hop(2, k, by).start()
+                p.to_owner().start()
 
     down_gather.forward(0)
     down_gather.third()
+    compute(groups[2])
+    compute(groups[1])
+    combine(groups[2])
+    down_gather.forward(1)
+    down_gather.fourth()
     compute(groups[0])
-    compute(groups[1])
+    combine(groups[1])
+    compute(groups[4])
     combine(groups[0])
-    combine(groups[1])
-    down_gather.forward(1)
-    compute(groups[2])
-    relay(groups[0])
+    down_gather.last(0)
     compute(groups[3])
-    relay(groups[1])
-    combine(groups[2])
+    combine(groups[4])
     combine(groups[3])
-    deliver(groups[0])
-    deliver(groups[1])
     down_gather.forward(2)
-    relay(groups[2])
-    relay(groups[3])
+    compute(groups[6])
+    combine(groups[6])
+    down_gather.last(1)
+    compute(groups[5])
+    combine(groups[5])
     down_gather.forward(3)
-    compute(groups[4])
-    deliver(groups[2])
-    compute(groups[5])
-    combine(groups[4])
-    combine(groups[5])
-    deliver(groups[3])
-    down_gather.last(0)
-    down_gather.last(1)
-    compute(groups[6])
-    relay(groups[4])
-    relay(groups[5])
-    combine(groups[6])
-    deliver(groups[4])
-    deliver(groups[5])
+    compute(groups[8])
+    combine(groups[8])
     down_gather.last(2)
+    compute(groups[7])
+    combine(groups[7])
     down_gather.last(3)
-    compute(groups[7])
-    relay(groups[6])
-    combine(groups[7])
-    deliver(groups[6])
-    relay(groups[7])
-    deliver(groups[7])
+    compute(groups[9])
+    combine(groups[9])
 
     for copy in sq_copies:
         copy.wait_recv()
@@ -537,8 +499,9 @@
         p.pair = y * 4 + part
     for p in own:
         p.to_pair().wait_recv()
-        for k, by in DIRS:
-            p.hop(2, k, by).wait_recv()
+        for away in (1, 2, 3):
+            p.away = away
+            p.to_owner().wait_recv()
     mine = pl.ds(pl.multiple_of((y * 4 + c * 2) * SHARD, FEATURES), FEATURES)
     beside = pl.ds(pl.multiple_of(y * FEATURES, FEATURES), FEATURES)
 
@@ -546,15 +509,14 @@
     def _(i):
         tokens = pl.ds(pl.multiple_of(i * 128, 128), 128)
         total = partials[mine, tokens].astype(F32) + paired[beside, tokens].astype(F32)
-        total = total + final[:, tokens].astype(F32)
+        for k in range(3):
+            total = total + final[k * FEATURES : (k + 1) * FEATURES, tokens].astype(F32)
         norm = squares[0:1, tokens]
         for k in range(1, 8):
             norm = norm + squares[8 * k : 8 * k + 1, tokens]
         total = total * (1.0 / (norm * (1.0 / D) + EPSILON))
-        out_v[tokens, :] = (stream[tokens, :].astype(F32) + jnp.transpose(total)).astype(BF16)
-
-    store = pltpu.make_async_copy(out_v, result, local_sem.at[7])
-    store.start()
+        result[tokens, :] = (stream[tokens, :].astype(F32) + jnp.transpose(total)).astype(BF16)
+
     for copy in pending:
         copy.wait_send()
     for k in range(16):
@@ -562,10 +524,9 @@
         p.pair = k
         p.to_pair().wait_send()
     for p in own:
-        for k, by in DIRS:
-            for step in range(3):
-                p.hop(step, k, by).wait_send()
-    store.wait()
+        for away in (1, 2, 3):
+            p.away = away
+            p.to_owner().wait_send()
 
 
 def body(
@@ -576,10 +537,9 @@
     dma = pltpu.SemaphoreType.DMA
     return pl.pallas_call(
         kernel,
-        out_shape=jax.ShapeDtypeStruct((ROWS, FEATURES), BF16),
-        in_specs=[hbm, hbm, hbm, pl.BlockSpec(memory_space=pltpu.SMEM), hbm, hbm,
-                  pl.BlockSpec(memory_space=pltpu.VMEM), hbm, hbm],
-        out_specs=hbm,
+        out_shape=pltpu.VMEM((ROWS, FEATURES), BF16),
+        in_specs=[hbm] * 9,
+        out_specs=pl.BlockSpec(memory_space=pltpu.VMEM),
         scratch_shapes=[
             pltpu.VMEM((D, HIDDEN), BF16),
             pltpu.VMEM((D, HIDDEN), BF16),
@@ -599,16 +559,16 @@
             pltpu.VMEM((HEAD_SIZE, WINDOW), BF16),
             pltpu.VMEM((D, ROWS), BF16),
             pltpu.VMEM((D // 2, ROWS), BF16),
-            pltpu.VMEM((16 * QUARTER, ROWS), BF16),
-            pltpu.VMEM((FEATURES, ROWS), BF16),
+            pltpu.VMEM((3 * FEATURES, ROWS), BF16),
             pltpu.VMEM((64, ROWS), F32),
-            pltpu.VMEM((ROWS, FEATURES), BF16),
-            dma((8,)), dma((11,)), dma((11,)), dma((2,)), dma((2,)), dma((80,)), dma((80,)),
+            pltpu.SMEM((3,), F32),
+            pltpu.VMEM((FEATURES,), BF16),
+            dma((9,)), dma((11,)), dma((11,)), dma((2,)), dma((2,)), dma((80,)), dma((80,)),
             dma((8,)), dma((8,)), dma((10,)), dma((10,)), dma((7,)), dma((7,)),
-            dma((16,)), dma((16,)), dma((24,)), dma((24,)),
+            dma((16,)), dma((16,)), dma((12,)), dma((12,)),
         ],
         compiler_params=pltpu.CompilerParams(
-            collective_id=0, has_side_effects=True, vmem_limit_bytes=67043328
+            collective_id=0, has_side_effects=True, vmem_limit_bytes=60 * 2**20
         ),
     )(
         queries.T, key_heads.T, projected_value_heads.T, sink_logit_table, out_weight,

time: 135 us -> 126 us (0.933)
  Pallas kernels: 132 us -> 124 us
    pallas_call x1, Pallas kernels: 132 us -> 124 us  [body(): pl.pallas_call(kernel, out_shape=pltpu.VMEM((ROWS, FEATURES), BF16), in_s...]
where the time goes in v3:
time: 126 us; the launch traced here: 125 us
  Pallas kernels  124 us (98%)
    pallas_call x1, Pallas kernels, body(): pl.pallas_call(kernel, out_shape=pltpu.VMEM((ROWS, FEATURES), BF16), in_s...  124 us

profile of v3, /device:TPU:9, one launch (start us, length us, event | category | flops | bytes accessed | tf_op | source)
XLA Modules:
  0.0 125.3 jit_solution(9291528100584164820)
XLA Ops:
  0.0 124.4 %shard_map.91 = bf16[1024,384]{1,0:T(8,128)(2,1)S(1)} custom-call(bf16[192,1024]{1,0:T(8,128)(2,1)} %bitcast.5, bf16[64,1024]{1,0:T(8,128)(2,1)} %bitcast.6, bf16[64,1024]{1,0:T(8,128)(2,1)} %bitcast.7, f32[3]{0:T(128)} %sinks_in.1, bf16[192,3072]{1,0:T(8,128)(2,1)} %out_weight.1, bf16[1024,384]{1,0:T(8,128)(2,1)} %residual.1, bf16[384]{0:T(512)(128)(2,1)} %gains_in.1, ...), custom_call_target="tpu_custom_call" | custom-call | tf_op jit(solution)/shard_map/pallas_call | solution.py:538
  124.4 0.9 copy.11

commit v4 on v3

--- a/solution.py
+++ b/solution.py
@@ -34,10 +34,10 @@
     queries, keys, values, sinks_in, out_weight, residual, gains_in, up, down,
     result,
     up_all, down_all, x_all, att_all, w_all, w_pass, hidden, act_t, mixed, stream, res_v,
-    q_v, k_v, v_v, halo_k, halo_v, partials, paired, final, squares, sink, gain,
+    q_v, k_v, v_v, halo_k, halo_v, partials, paired, chained, final, squares, sink, gain,
     local_sem, w_send, w_recv, halo_send, halo_recv, g_send, g_recv,
     att_send, att_recv, x_send, x_recv, sq_send, sq_recv,
-    pair_send, pair_recv, owner_send, owner_recv,
+    pair_send, pair_recv, side_send, side_recv, owner_send, owner_recv,
 ):
     s, t = lax.axis_index("sp"), lax.axis_index("tp")
     z, x = s // 4, s % 4
@@ -150,15 +150,16 @@
             sec, prim = self.at(half)
             for d, by in DIRS:
                 self.wait(half, 2 + d, sec, ring(prim, 2), d * QUARTER, QUARTER)
-            self.spread(half, 3)
 
         def third(self):
             self.spread(0, 2)
             self.opposite(1)
+            self.spread(1, 3)
+            self.opposite(0)
 
         def fourth(self):
             self.spread(1, 2)
-            self.opposite(0)
+            self.spread(0, 3)
 
         def forward(self, k):
             for half in (0, 1):
@@ -245,11 +246,140 @@
         copy.wait()
     sinks = jnp.concatenate([jnp.full((1, WINDOW), sink[g], F32) for g in range(3)], axis=1)
 
-    @pl.loop(1, 8)
-    def _(n):
-        band = pl.ds(pl.multiple_of((n - 1) * WINDOW, WINDOW), 2 * WINDOW)
-        attend(n, k_v[:, band], v_v[:, band], near)
-
+    def attend_blocks(low, high):
+        @pl.loop(low, high)
+        def _(n):
+            band = pl.ds(pl.multiple_of((n - 1) * WINDOW, WINDOW), 2 * WINDOW)
+            attend(n, k_v[:, band], v_v[:, band], near)
+
+    PART = ROWS // 2
+    FIRST = (PART, 0)
+
+    def att_rows(yy, cc, part, low=0, count=HEADS):
+        row = (yy * 2 + cc) * HEADS + low
+        return att_all.at[pl.ds(pl.multiple_of(row, 32), count), pl.ds(FIRST[part], PART)]
+
+    def att_copy(part, index, ref, target):
+        k = part * 8 + index
+        return remote(ref, ref, att_send.at[k], att_recv.at[k], target)
+
+    def att_arrived(part, index, ref):
+        att_copy(part, index, ref, partner).wait_recv()
+
+    def att_begin(part):
+        for d, by in DIRS:
+            start(att_copy(part, d, att_rows(y, c, part), y_next[by]))
+
+    def att_pass(part):
+        for d, by in DIRS:
+            near_y = ring(y, -by)
+            att_arrived(part, d, att_rows(near_y, c, part))
+            start(att_copy(part, 2 + d, att_rows(near_y, c, part, d * HALF, HALF), y_next[by]))
+            start(att_copy(part, 5 + d, att_rows(near_y, c, part), partner))
+
+    def mix(yy, part, first):
+        rows = pl.ds(pl.multiple_of(yy * 2 * HEADS, 2 * HEADS), 2 * HEADS)
+
+        @pl.loop(0, PART // TILE)
+        def _(i):
+            tokens = pl.ds(pl.multiple_of(FIRST[part] + i * TILE, TILE), TILE)
+            total = dot(att_all[rows, tokens], w_all[rows, :], ((0,), (0,)))
+            mixed[tokens, :] = total if first else mixed[tokens, :] + total
+
+    def mix_near(part):
+        for d, by in DIRS:
+            near_y = ring(y, -by)
+            att_arrived(part, 5 + d, att_rows(near_y, 1 - c, part))
+            if part == 0:
+                for cc in (0, 1):
+                    w_arrived(1 + 2 * d + cc, w_rows(near_y, cc))
+            mix(near_y, part, False)
+
+    def mix_far(part):
+        far = ring(y, 2)
+        for d, by in DIRS:
+            att_arrived(part, 2 + d, att_rows(far, c, part, d * HALF, HALF))
+        start(att_copy(part, 7, att_rows(far, c, part), partner))
+        if part == 0:
+            for d, by in DIRS:
+                for cc in (0, 1):
+                    w_arrived(7 + 2 * d + cc, w_rows(far, cc, d * HALF, HALF))
+        att_arrived(part, 7, att_rows(far, 1 - c, part))
+        mix(far, part, False)
+
+    lanes_of = lambda cc: pl.ds(pl.multiple_of(cc * FEATURES, 128), FEATURES)
+
+    def x_block(yy, cc, part, quarter=None):
+        low, count = (0, PART) if quarter is None else (quarter * TILE, TILE)
+        return x_all.at[pl.ds(pl.multiple_of(yy * ROWS + FIRST[part] + low, TILE), count), lanes_of(cc)]
+
+    ones = jnp.ones((8, FEATURES), BF16)
+    sq_rows = pl.ds(pl.multiple_of(t * 8, 8), 8)
+
+    def make_x(part):
+        gains = gain[...].astype(F32).reshape(1, FEATURES)
+
+        @pl.loop(0, PART // TILE)
+        def _(i):
+            tokens = pl.ds(pl.multiple_of(FIRST[part] + i * TILE, TILE), TILE)
+            here = (res_v[tokens, :].astype(F32) + mixed[tokens, :]).astype(BF16)
+            stream[tokens, :] = here
+            wide = here.astype(F32)
+            rows = pl.ds(pl.multiple_of(y * ROWS + FIRST[part] + i * TILE, TILE), TILE)
+            x_all[rows, lanes_of(c)] = (wide * gains).astype(BF16)
+            sq = wide * wide
+            high = sq.astype(BF16)
+            low = (sq - high.astype(F32)).astype(BF16)
+            squares[sq_rows, tokens] = dot(ones, high, ((1,), (1,))) + dot(ones, low, ((1,), (1,)))
+
+    def x_copy(part, index, ref, target):
+        k = part * 10 + index
+        return remote(ref, ref, x_send.at[k], x_recv.at[k], target)
+
+    def x_arrived(part, index, ref):
+        x_copy(part, index, ref, partner).wait_recv()
+
+    def x_begin(part, second):
+        for d, by in DIRS:
+            quarter = 1 - d if second else d
+            start(x_copy(part, 2 * second + d, x_block(y, c, part, quarter), y_next[by]))
+
+    def x_pass(part):
+        for d, by in DIRS:
+            ref = x_block(ring(y, -by), c, part, d)
+            x_arrived(part, d, ref)
+            start(x_copy(part, 4 + d, ref, y_next[by]))
+
+    def x_near(part):
+        for d, by in DIRS:
+            x_arrived(part, 2 + d, x_block(ring(y, -by), c, part, 1 - d))
+            start(x_copy(part, 7 + d, x_block(ring(y, -by), c, part), partner))
+
+    def x_far(part):
+        for d, by in DIRS:
+            x_arrived(part, 4 + d, x_block(ring(y, 2), c, part, d))
+        start(x_copy(part, 9, x_block(ring(y, 2), c, part), partner))
+
+    def hide(yy, part, first=False, last=False):
+        @pl.loop(0, PART // TILE)
+        def _(i):
+            tokens = pl.ds(pl.multiple_of(FIRST[part] + i * TILE, TILE), TILE)
+            rows = pl.ds(pl.multiple_of(yy * ROWS + FIRST[part] + i * TILE, TILE), TILE)
+            for n in range(3):
+                cols = pl.ds(n * 512, 512)
+                total = dot(x_all[rows, :], up_all[pl.ds(pl.multiple_of(yy * 768, 768), 768), cols], ((1,), (0,)))
+                if not first:
+                    total = total + hidden[tokens, cols]
+                if last:
+                    units = jnp.square(jnp.maximum(total, 0.0)).astype(BF16)
+                    act_t[cols, tokens] = jnp.transpose(units)
+                else:
+                    hidden[tokens, cols] = total
+
+    attend_blocks(4, 8)
+    att_begin(0)
+    start(att_copy(0, 4, att_rows(y, c, 0), partner))
+    attend_blocks(1, 4)
     for copy in halo_copies:
         copy.wait_recv()
     first_key = jnp.where(s == 0, WINDOW, 0)
@@ -259,142 +389,73 @@
         jnp.concatenate([halo_v[...], v_v[:, 0:WINDOW]], axis=1),
         near & (key_at >= first_key),
     )
-
-    def att_rows(yy, cc, low=0, count=HEADS):
-        row = (yy * 2 + cc) * HEADS + low
-        return att_all.at[pl.ds(pl.multiple_of(row, 32), count)]
-
-    def att_copy(index, ref, target):
-        return remote(ref, ref, att_send.at[index], att_recv.at[index], target)
-
-    def att_arrived(index, ref):
-        att_copy(index, ref, partner).wait_recv()
-
-    for d, by in DIRS:
-        start(att_copy(d, att_rows(y, c), y_next[by]))
-    start(att_copy(4, att_rows(y, c), partner))
+    start(att_copy(1, 4, att_rows(y, c, 1), partner))
     w_pass_on()
     up_gather.second()
-
     for copy in locals_[4:]:
         copy.wait()
-
-    def mix(yy, first):
-        rows = pl.ds(pl.multiple_of(yy * 2 * HEADS, 2 * HEADS), 2 * HEADS)
-
-        @pl.loop(0, ROWS // TILE)
-        def _(i):
-            tokens = pl.ds(pl.multiple_of(i * TILE, TILE), TILE)
-            part = dot(att_all[rows, tokens], w_all[rows, :], ((0,), (0,)))
-            mixed[tokens, :] = part if first else mixed[tokens, :] + part
-
-    att_arrived(4, att_rows(y, 1 - c))
     w_arrived(0, w_rows(y, 1 - c))
-    mix(y, True)
+    for part in (0, 1):
+        att_arrived(part, 4, att_rows(y, 1 - c, part))
+        mix(y, part, True)
+    att_pass(0)
+    att_begin(1)
     up_gather.forward(0)
     up_gather.third()
-    for d, by in DIRS:
-        att_arrived(d, att_rows(ring(y, -by), c))
-        start(att_copy(2 + d, att_rows(ring(y, -by), c, d * HALF, HALF), y_next[by]))
-        start(att_copy(5 + d, att_rows(ring(y, -by), c), partner))
-    for d, by in DIRS:
-        att_arrived(5 + d, att_rows(ring(y, -by), 1 - c))
-        for cc in (0, 1):
-            w_arrived(1 + 2 * d + cc, w_rows(ring(y, -by), cc))
-        mix(ring(y, -by), False)
+    mix_near(0)
+    mix_far(0)
+    make_x(0)
+    x_begin(0, False)
+    att_pass(1)
+    x_begin(0, True)
+    start(x_copy(0, 6, x_block(y, c, 0), partner))
     up_gather.forward(1)
     up_gather.fourth()
-    for d, by in DIRS:
-        att_arrived(2 + d, att_rows(ring(y, 2), c, d * HALF, HALF))
-    start(att_copy(7, att_rows(ring(y, 2), c), partner))
-    att_arrived(7, att_rows(ring(y, 2), 1 - c))
-    for d, by in DIRS:
-        for cc in (0, 1):
-            w_arrived(7 + 2 * d + cc, w_rows(ring(y, 2), cc, d * HALF, HALF))
-    mix(ring(y, 2), False)
-
-    lanes_of = lambda cc: pl.ds(pl.multiple_of(cc * FEATURES, 128), FEATURES)
-
-    def x_block(yy, cc, low=0, count=ROWS):
-        return x_all.at[pl.ds(pl.multiple_of(yy * ROWS + low, 512), count), lanes_of(cc)]
-
-    gains = gain[...].astype(F32).reshape(1, FEATURES)
-    ones = jnp.ones((8, FEATURES), BF16)
-    sq_rows = pl.ds(pl.multiple_of(t * 8, 8), 8)
-
-    @pl.loop(0, ROWS // TILE)
-    def _(i):
-        tokens = pl.ds(pl.multiple_of(i * TILE, TILE), TILE)
-        here = (res_v[tokens, :].astype(F32) + mixed[tokens, :]).astype(BF16)
-        stream[tokens, :] = here
-        wide = here.astype(F32)
-        x_all[pl.ds(pl.multiple_of(y * ROWS + i * TILE, TILE), TILE), lanes_of(c)] = (wide * gains).astype(BF16)
-        sq = wide * wide
-        high = sq.astype(BF16)
-        low = (sq - high.astype(F32)).astype(BF16)
-        squares[sq_rows, tokens] = dot(ones, high, ((1,), (1,))) + dot(ones, low, ((1,), (1,)))
-
-    def x_copy(index, ref, target):
-        return remote(ref, ref, x_send.at[index], x_recv.at[index], target)
-
-    def x_arrived(index, ref):
-        x_copy(index, ref, partner).wait_recv()
-
-    for part in (0, 1):
-        for d, by in DIRS:
-            start(x_copy(2 * part + d, x_block(y, c, part * 512, 512), y_next[by]))
-    start(x_copy(6, x_block(y, c), partner))
+    mix_near(1)
+    x_pass(0)
+    mix_far(1)
+    make_x(1)
+    x_begin(1, False)
+    x_begin(1, True)
+    start(x_copy(1, 6, x_block(y, c, 1), partner))
     sq_copies = []
     for k in range(1, 8):
         ref = squares.at[sq_rows]
         copy = remote(ref, ref, sq_send.at[k - 1], sq_recv.at[k - 1], (s, (t + k) % 8))
         start(copy)
         sq_copies.append(copy)
-
+    x_near(0)
     up_gather.forward(2)
-    x_arrived(0, x_block(ring(y, -1), c, 0, 512))
-    start(x_copy(4, x_block(ring(y, -1), c, 0, 512), y_next[1]))
-    x_arrived(1, x_block(ring(y, 1), c, 0, 512))
+    x_far(0)
+    up_gather.last(0)
+    x_arrived(0, 6, x_block(y, 1 - c, 0))
+    for d, by in DIRS:
+        x_arrived(0, 7 + d, x_block(ring(y, -by), 1 - c, 0))
+    x_arrived(0, 9, x_block(ring(y, 2), 1 - c, 0))
+    hide(z, 0, first=True)
     up_gather.forward(3)
     down_gather.first()
-    x_arrived(3, x_block(ring(y, 1), c, 512, 512))
-    start(x_copy(5, x_block(ring(y, 1), c, 512, 512), y_next[-1]))
-    x_arrived(2, x_block(ring(y, -1), c, 512, 512))
-    start(x_copy(7, x_block(ring(y, -1), c), partner))
-    start(x_copy(8, x_block(ring(y, 1), c), partner))
-
-    def hide(yy, first, last):
-        @pl.loop(0, ROWS // TILE)
-        def _(i):
-            tokens = pl.ds(pl.multiple_of(i * TILE, TILE), TILE)
-            block = x_all[pl.ds(pl.multiple_of(yy * ROWS + i * TILE, TILE), TILE), :]
-            for n in range(3):
-                cols = pl.ds(n * 512, 512)
-                part = dot(block, up_all[pl.ds(pl.multiple_of(yy * 768, 768), 768), cols], ((1,), (0,)))
-                if not first:
-                    part = part + hidden[tokens, cols]
-                if last:
-                    units = jnp.square(jnp.maximum(part, 0.0)).astype(BF16)
-                    act_t[cols, tokens] = jnp.transpose(units)
-                else:
-                    hidden[tokens, cols] = part
-
-    for j in range(4):
-        up_gather.last(j)
-    x_arrived(6, x_block(y, 1 - c))
-    hide(y, True, False)
+    x_pass(1)
+    up_gather.last(1)
+    hide(ring(z, -1), 0)
+    x_near(1)
+    up_gather.last(2)
+    up_gather.last(3)
+    hide(ring(z, 1), 0)
+    hide(ring(z, 2), 0, last=True)
+    x_far(1)
+    x_arrived(1, 6, x_block(y, 1 - c, 1))
+    hide(y, 1, first=True)
     for d, by in DIRS:
-        x_arrived(7 + d, x_block(ring(y, -by), 1 - c))
-        hide(ring(y, -by), False, False)
+        x_arrived(1, 7 + d, x_block(ring(y, -by), 1 - c, 1))
+        hide(ring(y, -by), 1)
         if d == 0:
             down_gather.second()
-    x_arrived(4, x_block(ring(y, 2), c, 0, 512))
-    x_arrived(5, x_block(ring(y, 2), c, 512, 512))
-    start(x_copy(9, x_block(ring(y, 2), c), partner))
-    x_arrived(9, x_block(ring(y, 2), 1 - c))
-    hide(ring(y, 2), False, True)
-
-    GROUPS = [[(half, 0, j) for j in range(4)] for half in (0, 1)]
+    x_arrived(1, 9, x_block(ring(y, 2), 1 - c, 1))
+    hide(ring(y, 2), 1, last=True)
+
+    GROUPS = [[(half, 0, j) for j in range(3)] for half in (0, 1)]
+    GROUPS.append([(half, 0, 3) for half in (0, 1)])
     for k in range(4):
         GROUPS.append([(half, i, ORDER[half][k]) for half in (0, 1) for i in (1, 2)])
         GROUPS.append([(half, 3, ORDER[half][k]) for half in (0, 1)])
@@ -405,6 +466,7 @@
             sec, prim = ring(sec, STEPS[i]), ring(prim, STEPS[j])
             zz, xx = (sec, prim) if half == 0 else (prim, sec)
             self.row = (zz * 4 + xx) * SHARD + half * HALF
+            self.half = half
             self.part = (xx % 2) * 2 + half
             self.mine = xx // 2 == c
             self.away = (y - zz + 4) % 4
@@ -422,17 +484,27 @@
                 pair_send.at[self.pair], pair_recv.at[self.pair], partner,
             )
 
+        def to_side(self):
+            return remote(
+                partials.at[self.rows()], chained.at[pl.ds(pl.multiple_of(self.part * HALF, 32), HALF)],
+                side_send.at[self.part], side_recv.at[self.part], y_next[-1 if self.half == 0 else 1],
+            )
+
         def to_owner(self):
-            index = (self.away - 1) * 4 + self.part
+            index = (self.away // 2) * 4 + self.part
             return remote(
                 partials.at[self.rows()], final.at[pl.ds(pl.multiple_of(index * HALF, 32), HALF)],
                 owner_send.at[index], owner_recv.at[index], (s, ring(y, -self.away) * 2 + c),
             )
 
-        def add_pair(self, k):
-            rows = self.rows(k * QUARTER, QUARTER)
-            total = partials[rows, :].astype(F32) + paired[self.paired_rows(k * QUARTER, QUARTER), :].astype(F32)
-            partials[rows, :] = total.astype(BF16)
+        def add(self, side):
+            for k in (0, 1):
+                rows = self.rows(k * QUARTER, QUARTER)
+                total = partials[rows, :].astype(F32) + paired[self.paired_rows(k * QUARTER, QUARTER), :].astype(F32)
+                if side:
+                    there = pl.ds(pl.multiple_of(self.part * HALF + k * QUARTER, 16), QUARTER)
+                    total = total + chained[there, :].astype(F32)
+                partials[rows, :] = total.astype(BF16)
 
     groups = [[Piece(*facts) for facts in group] for group in GROUPS]
 
@@ -452,54 +524,85 @@
 
     def combine(group):
         for p in group:
-            @pl.when(p.mine & (p.away != 0))
+            side = 1 if p.half == 0 else 3
+
+            @pl.when(p.mine & (p.away != 0) & (p.away != side))
             def _():
                 p.to_pair().wait_recv()
-                for k in (0, 1):
-                    p.add_pair(k)
+                p.add(False)
+
+                @pl.when(p.away == 2)
+                def _():
+                    p.to_side().start()
+
+                @pl.when(p.away != 2)
+                def _():
+                    p.to_owner().start()
+
+    def relay(group):
+        for p in group:
+            @pl.when(p.mine & (p.away == (1 if p.half == 0 else 3)))
+            def _():
+                p.to_pair().wait_recv()
+                p.to_side().wait_recv()
+                p.add(True)
                 p.to_owner().start()
 
+    compute(groups[0])
+    compute(groups[1])
+    combine(groups[0])
     down_gather.forward(0)
+    compute(groups[3])
+    combine(groups[1])
     down_gather.third()
     compute(groups[2])
-    compute(groups[1])
+    combine(groups[3])
     combine(groups[2])
     down_gather.forward(1)
     down_gather.fourth()
-    compute(groups[0])
-    combine(groups[1])
+    compute(groups[5])
+    relay(groups[0])
+    relay(groups[1])
+    down_gather.last(0)
+    combine(groups[5])
     compute(groups[4])
-    combine(groups[0])
-    down_gather.last(0)
-    compute(groups[3])
     combine(groups[4])
-    combine(groups[3])
+    relay(groups[3])
     down_gather.forward(2)
+    compute(groups[7])
+    relay(groups[2])
+    combine(groups[7])
+    down_gather.last(1)
     compute(groups[6])
     combine(groups[6])
-    down_gather.last(1)
-    compute(groups[5])
-    combine(groups[5])
+    relay(groups[5])
+    relay(groups[4])
     down_gather.forward(3)
+    compute(groups[9])
+    combine(groups[9])
+    relay(groups[7])
+    down_gather.last(2)
     compute(groups[8])
     combine(groups[8])
-    down_gather.last(2)
-    compute(groups[7])
-    combine(groups[7])
+    relay(groups[6])
     down_gather.last(3)
-    compute(groups[9])
-    combine(groups[9])
+    compute(groups[10])
+    combine(groups[10])
+    relay(groups[9])
+    relay(groups[8])
+    relay(groups[10])
 
     for copy in sq_copies:
         copy.wait_recv()
     own = [Piece(half, 0, 0) for half in (0, 1, 0, 1)]
     for part, p in enumerate(own):
         p.part = part
+        p.half = part % 2
         p.row = (y * 4 + c * 2) * SHARD + part * HALF
         p.pair = y * 4 + part
     for p in own:
         p.to_pair().wait_recv()
-        for away in (1, 2, 3):
+        for away in (1, 3):
             p.away = away
             p.to_owner().wait_recv()
     mine = pl.ds(pl.multiple_of((y * 4 + c * 2) * SHARD, FEATURES), FEATURES)
@@ -509,7 +612,7 @@
     def _(i):
         tokens = pl.ds(pl.multiple_of(i * 128, 128), 128)
         total = partials[mine, tokens].astype(F32) + paired[beside, tokens].astype(F32)
-        for k in range(3):
+        for k in range(2):
             total = total + final[k * FEATURES : (k + 1) * FEATURES, tokens].astype(F32)
         norm = squares[0:1, tokens]
         for k in range(1, 8):
@@ -524,7 +627,8 @@
         p.pair = k
         p.to_pair().wait_send()
     for p in own:
-        for away in (1, 2, 3):
+        p.to_side().wait_send()
+        for away in (1, 3):
             p.away = away
             p.to_owner().wait_send()
 
@@ -559,13 +663,14 @@
             pltpu.VMEM((HEAD_SIZE, WINDOW), BF16),
             pltpu.VMEM((D, ROWS), BF16),
             pltpu.VMEM((D // 2, ROWS), BF16),
-            pltpu.VMEM((3 * FEATURES, ROWS), BF16),
+            pltpu.VMEM((FEATURES, ROWS), BF16),
+            pltpu.VMEM((2 * FEATURES, ROWS), BF16),
             pltpu.VMEM((64, ROWS), F32),
             pltpu.SMEM((3,), F32),
             pltpu.VMEM((FEATURES,), BF16),
             dma((9,)), dma((11,)), dma((11,)), dma((2,)), dma((2,)), dma((80,)), dma((80,)),
-            dma((8,)), dma((8,)), dma((10,)), dma((10,)), dma((7,)), dma((7,)),
-            dma((16,)), dma((16,)), dma((12,)), dma((12,)),
+            dma((16,)), dma((16,)), dma((20,)), dma((20,)), dma((7,)), dma((7,)),
+            dma((16,)), dma((16,)), dma((4,)), dma((4,)), dma((8,)), dma((8,)),
         ],
         compiler_params=pltpu.CompilerParams(
             collective_id=0, has_side_effects=True, vmem_limit_bytes=60 * 2**20

time: 126 us -> 122 us (0.968)
  Pallas kernels: 124 us -> 120 us
    pallas_call x1, Pallas kernels: 124 us -> 120 us  [body(): pl.pallas_call(kernel, out_shape=pltpu.VMEM((ROWS, FEATURES), BF16), in_s...]
where the time goes in v4:
time: 122 us; the launch traced here: 121 us
  Pallas kernels  120 us (98%)
    pallas_call x1, Pallas kernels, body(): pl.pallas_call(kernel, out_shape=pltpu.VMEM((ROWS, FEATURES), BF16), in_s...  120 us

profile of v4, /device:TPU:9, one launch (start us, length us, event | category | flops | bytes accessed | tf_op | source)
XLA Modules:
  0.0 121.2 jit_solution(11402827231543730593)
XLA Ops:
  0.0 120.3 %shard_map.91 = bf16[1024,384]{1,0:T(8,128)(2,1)S(1)} custom-call(bf16[192,1024]{1,0:T(8,128)(2,1)} %bitcast.5, bf16[64,1024]{1,0:T(8,128)(2,1)} %bitcast.6, bf16[64,1024]{1,0:T(8,128)(2,1)} %bitcast.7, f32[3]{0:T(128)} %sinks_in.1, bf16[192,3072]{1,0:T(8,128)(2,1)} %out_weight.1, bf16[1024,384]{1,0:T(8,128)(2,1)} %residual.1, bf16[384]{0:T(512)(128)(2,1)} %gains_in.1, ...), custom_call_target="tpu_custom_call" | custom-call | tf_op jit(solution)/shard_map/pallas_call | solution.py:642
  120.3 0.9 copy.11

commit v5 on v4

--- a/solution.py
+++ b/solution.py
@@ -460,6 +460,9 @@
         GROUPS.append([(half, i, ORDER[half][k]) for half in (0, 1) for i in (1, 2)])
         GROUPS.append([(half, 3, ORDER[half][k]) for half in (0, 1)])
 
+    def lanes(part):
+        return pl.ds(pl.multiple_of(part * PART, PART), PART)
+
     class Piece:
         def __init__(self, half, i, j):
             sec, prim = down_gather.at(half)
@@ -478,75 +481,85 @@
         def paired_rows(self, low=0, count=HALF):
             return pl.ds(pl.multiple_of(self.pair * HALF + low, 16), count)
 
-        def to_pair(self):
+        def to_pair(self, part):
+            k = self.pair * 2 + part
             return remote(
-                partials.at[self.rows()], paired.at[self.paired_rows()],
-                pair_send.at[self.pair], pair_recv.at[self.pair], partner,
+                partials.at[self.rows(), lanes(part)], paired.at[self.paired_rows(), lanes(part)],
+                pair_send.at[k], pair_recv.at[k], partner,
             )
 
-        def to_side(self):
+        def to_side(self, part):
+            k = self.part * 2 + part
             return remote(
-                partials.at[self.rows()], chained.at[pl.ds(pl.multiple_of(self.part * HALF, 32), HALF)],
-                side_send.at[self.part], side_recv.at[self.part], y_next[-1 if self.half == 0 else 1],
+                partials.at[self.rows(), lanes(part)],
+                chained.at[pl.ds(pl.multiple_of(self.part * HALF, 32), HALF), lanes(part)],
+                side_send.at[k], side_recv.at[k], y_next[-1 if self.half == 0 else 1],
             )
 
-        def to_owner(self):
+        def to_owner(self, part):
             index = (self.away // 2) * 4 + self.part
+            k = index * 2 + part
             return remote(
-                partials.at[self.rows()], final.at[pl.ds(pl.multiple_of(index * HALF, 32), HALF)],
-                owner_send.at[index], owner_recv.at[index], (s, ring(y, -self.away) * 2 + c),
+                partials.at[self.rows(), lanes(part)],
+                final.at[pl.ds(pl.multiple_of(index * HALF, 32), HALF), lanes(part)],
+                owner_send.at[k], owner_recv.at[k], (s, ring(y, -self.away) * 2 + c),
             )
 
-        def add(self, side):
-            for k in (0, 1):
-                rows = self.rows(k * QUARTER, QUARTER)
-                total = partials[rows, :].astype(F32) + paired[self.paired_rows(k * QUARTER, QUARTER), :].astype(F32)
-                if side:
-                    there = pl.ds(pl.multiple_of(self.part * HALF + k * QUARTER, 16), QUARTER)
-                    total = total + chained[there, :].astype(F32)
-                partials[rows, :] = total.astype(BF16)
+        def add(self, part, side):
+            rows = self.rows()
+            total = partials[rows, lanes(part)].astype(F32) + paired[self.paired_rows(), lanes(part)].astype(F32)
+            if side:
+                there = pl.ds(pl.multiple_of(self.part * HALF, 32), HALF)
+                total = total + chained[there, lanes(part)].astype(F32)
+            partials[rows, lanes(part)] = total.astype(BF16)
 
     groups = [[Piece(*facts) for facts in group] for group in GROUPS]
 
     def compute(group):
-        @pl.loop(0, ROWS // TILE)
-        def _(i):
-            tokens = pl.ds(pl.multiple_of(i * TILE, TILE), TILE)
-            weight = jnp.concatenate([down_all[p.rows(), :] for p in group], axis=0)
-            part = dot(weight, act_t[:, tokens], ((1,), (0,))).astype(BF16)
-            for k, p in enumerate(group):
-                partials[p.rows(), tokens] = part[k * HALF : (k + 1) * HALF]
-
-        for p in group:
-            @pl.when(jnp.logical_not(p.mine))
-            def _():
-                p.to_pair().start()
+        @pl.loop(0, 2)
+        def _(part):
+            @pl.loop(0, PART // TILE)
+            def _(i):
+                tokens = pl.ds(pl.multiple_of(part * PART + i * TILE, TILE), TILE)
+                weight = jnp.concatenate([down_all[p.rows(), :] for p in group], axis=0)
+                total = dot(weight, act_t[:, tokens], ((1,), (0,))).astype(BF16)
+                for k, p in enumerate(group):
+                    partials[p.rows(), tokens] = total[k * HALF : (k + 1) * HALF]
+
+            for p in group:
+                @pl.when(jnp.logical_not(p.mine))
+                def _():
+                    p.to_pair(part).start()
 
     def combine(group):
-        for p in group:
-            side = 1 if p.half == 0 else 3
-
-            @pl.when(p.mine & (p.away != 0) & (p.away != side))
-            def _():
-                p.to_pair().wait_recv()
-                p.add(False)
-
-                @pl.when(p.away == 2)
+        @pl.loop(0, 2)
+        def _(part):
+            for p in group:
+                side = 1 if p.half == 0 else 3
+
+                @pl.when(p.mine & (p.away != 0) & (p.away != side))
                 def _():
-                    p.to_side().start()
-
-                @pl.when(p.away != 2)
+                    p.to_pair(part).wait_recv()
+                    p.add(part, False)
+
+                    @pl.when(p.away == 2)
+                    def _():
+                        p.to_side(part).start()
+
+                    @pl.when(p.away != 2)
+                    def _():
+                        p.to_owner(part).start()
+
+    def relay(group):
+        @pl.loop(0, 2)
+        def _(part):
+            for p in group:
+                @pl.when(p.mine & (p.away == (1 if p.half == 0 else 3)))
                 def _():
-                    p.to_owner().start()
-
-    def relay(group):
-        for p in group:
-            @pl.when(p.mine & (p.away == (1 if p.half == 0 else 3)))
-            def _():
-                p.to_pair().wait_recv()
-                p.to_side().wait_recv()
-                p.add(True)
-                p.to_owner().start()
+                    p.to_pair(part).wait_recv()
+                    p.to_side(part).wait_recv()
+                    p.add(part, True)
+                    p.to_owner(part).start()
 
     compute(groups[0])
     compute(groups[1])
@@ -600,37 +613,41 @@
         p.half = part % 2
         p.row = (y * 4 + c * 2) * SHARD + part * HALF
         p.pair = y * 4 + part
-    for p in own:
-        p.to_pair().wait_recv()
-        for away in (1, 3):
-            p.away = away
-            p.to_owner().wait_recv()
     mine = pl.ds(pl.multiple_of((y * 4 + c * 2) * SHARD, FEATURES), FEATURES)
     beside = pl.ds(pl.multiple_of(y * FEATURES, FEATURES), FEATURES)
 
-    @pl.loop(0, ROWS // 128)
-    def _(i):
-        tokens = pl.ds(pl.multiple_of(i * 128, 128), 128)
-        total = partials[mine, tokens].astype(F32) + paired[beside, tokens].astype(F32)
-        for k in range(2):
-            total = total + final[k * FEATURES : (k + 1) * FEATURES, tokens].astype(F32)
-        norm = squares[0:1, tokens]
-        for k in range(1, 8):
-            norm = norm + squares[8 * k : 8 * k + 1, tokens]
-        total = total * (1.0 / (norm * (1.0 / D) + EPSILON))
-        result[tokens, :] = (stream[tokens, :].astype(F32) + jnp.transpose(total)).astype(BF16)
+    @pl.loop(0, 2)
+    def _(part):
+        for p in own:
+            p.to_pair(part).wait_recv()
+            for away in (1, 3):
+                p.away = away
+                p.to_owner(part).wait_recv()
+
+        @pl.loop(0, PART // 128)
+        def _(i):
+            tokens = pl.ds(pl.multiple_of(part * PART + i * 128, 128), 128)
+            total = partials[mine, tokens].astype(F32) + paired[beside, tokens].astype(F32)
+            for k in range(2):
+                total = total + final[k * FEATURES : (k + 1) * FEATURES, tokens].astype(F32)
+            norm = squares[0:1, tokens]
+            for k in range(1, 8):
+                norm = norm + squares[8 * k : 8 * k + 1, tokens]
+            total = total * (1.0 / (norm * (1.0 / D) + EPSILON))
+            result[tokens, :] = (stream[tokens, :].astype(F32) + jnp.transpose(total)).astype(BF16)
 
     for copy in pending:
         copy.wait_send()
-    for k in range(16):
-        p = own[0]
-        p.pair = k
-        p.to_pair().wait_send()
-    for p in own:
-        p.to_side().wait_send()
-        for away in (1, 3):
-            p.away = away
-            p.to_owner().wait_send()
+    for part in (0, 1):
+        for k in range(16):
+            p = own[0]
+            p.pair = k
+            p.to_pair(part).wait_send()
+        for p in own:
+            p.to_side(part).wait_send()
+            for away in (1, 3):
+                p.away = away
+                p.to_owner(part).wait_send()
 
 
 def body(
@@ -670,7 +687,7 @@
             pltpu.VMEM((FEATURES,), BF16),
             dma((9,)), dma((11,)), dma((11,)), dma((2,)), dma((2,)), dma((80,)), dma((80,)),
             dma((16,)), dma((16,)), dma((20,)), dma((20,)), dma((7,)), dma((7,)),
-            dma((16,)), dma((16,)), dma((4,)), dma((4,)), dma((8,)), dma((8,)),
+            dma((32,)), dma((32,)), dma((8,)), dma((8,)), dma((16,)), dma((16,)),
         ],
         compiler_params=pltpu.CompilerParams(
             collective_id=0, has_side_effects=True, vmem_limit_bytes=60 * 2**20

time: 122 us -> 120 us (0.984)
    pallas_call x1, Pallas kernels: 120 us -> 119 us  [body(): pl.pallas_call(kernel, out_shape=pltpu.VMEM((ROWS, FEATURES), BF16), in_s...]
where the time goes in v5:
time: 120 us
  Pallas kernels  119 us (99%)
    pallas_call x1, Pallas kernels, body(): pl.pallas_call(kernel, out_shape=pltpu.VMEM((ROWS, FEATURES), BF16), in_s...  119 us

profile of v5, /device:TPU:9, one launch (start us, length us, event | category | flops | bytes accessed | tf_op | source)
XLA Modules:
  0.0 119.8 jit_solution(130872639185993165)
XLA Ops:
  0.0 118.9 %shard_map.91 = bf16[1024,384]{1,0:T(8,128)(2,1)S(1)} custom-call(bf16[192,1024]{1,0:T(8,128)(2,1)} %bitcast.5, bf16[64,1024]{1,0:T(8,128)(2,1)} %bitcast.6, bf16[64,1024]{1,0:T(8,128)(2,1)} %bitcast.7, f32[3]{0:T(128)} %sinks_in.1, bf16[192,3072]{1,0:T(8,128)(2,1)} %out_weight.1, bf16[1024,384]{1,0:T(8,128)(2,1)} %residual.1, bf16[384]{0:T(512)(128)(2,1)} %gains_in.1, ...), custom_call_target="tpu_custom_call" | custom-call | tf_op jit(solution)/shard_map/pallas_call | solution.py:659
  118.9 0.9 copy.11

commit v6 on v5

--- a/solution.py
+++ b/solution.py
@@ -59,11 +59,14 @@
             device_id=target, device_id_type=MESH,
         )
 
-    pending = []
-
     def start(copy):
         copy.start()
-        pending.append(copy)
+
+    def arrived(ref, sem):
+        remote(ref, ref, sem, sem, partner).wait_recv()
+
+    def sent(ref, sem):
+        remote(ref, ref, sem, sem, partner).wait_send()
 
     barrier = pltpu.get_barrier_semaphore()
     greeted = [
@@ -100,8 +103,14 @@
             return self.buf.at[pl.ds(pl.multiple_of(row, 16), count)]
 
         def copy(self, half, index, src, dst, target):
-            k = self.base + half * 20 + index
-            return remote(src, dst, g_send.at[k], g_recv.at[k], target)
+            if index < 4:
+                step = index // 2
+            else:
+                step = 2 + 4 * (index >= 12) + ORDER[half].index((index - 4) // 2 % 4)
+            return remote(src, dst, g_send.at[self.base], g_recv.at[self.base * 10 + step], target)
+
+        def arrived(self, step, rows):
+            arrived(self.buf.at[pl.ds(0, rows)], g_recv.at[self.base * 10 + step])
 
         def at(self, half):
             return (z, x) if half == 0 else (x, z)
@@ -125,16 +134,12 @@
                 for d, by in DIRS:
                     start(self.copy(half, 4 + d, src, dst, self.towards(half, False, by)))
 
-        def wait(self, half, index, sec, prim, low, count):
-            ref = self.spot(half, sec, prim, low, count)
-            self.copy(half, index, ref, ref, partner).wait_recv()
-
         def second(self):
+            self.arrived(0, 4 * HALF)
             for half in (0, 1):
                 sec, prim = self.at(half)
                 for d, by in DIRS:
                     origin = ring(prim, -by)
-                    self.wait(half, d, sec, origin, 0, HALF)
                     piece = self.spot(half, sec, origin, d * QUARTER, QUARTER)
                     start(self.copy(half, 2 + d, piece, piece, self.towards(half, True, by)))
             for half in (0, 1):
@@ -146,41 +151,33 @@
             for d, by in DIRS:
                 start(self.copy(half, 4 + 2 * j + d, piece, piece, self.towards(half, False, by)))
 
-        def opposite(self, half):
-            sec, prim = self.at(half)
-            for d, by in DIRS:
-                self.wait(half, 2 + d, sec, ring(prim, 2), d * QUARTER, QUARTER)
-
         def third(self):
             self.spread(0, 2)
-            self.opposite(1)
+            self.arrived(1, 4 * QUARTER)
             self.spread(1, 3)
-            self.opposite(0)
 
         def fourth(self):
             self.spread(1, 2)
             self.spread(0, 3)
 
         def forward(self, k):
+            self.arrived(2 + k, 4 * HALF)
             for half in (0, 1):
                 j = ORDER[half][k]
                 sec, prim = self.at(half)
                 origin = ring(prim, STEPS[j])
                 for d, by in DIRS:
-                    self.wait(half, 4 + 2 * j + d, ring(sec, -by), origin, 0, HALF)
                     piece = self.spot(half, ring(sec, -by), origin, d * QUARTER, QUARTER)
                     start(self.copy(half, 12 + 2 * j + d, piece, piece, self.towards(half, False, by)))
 
         def last(self, k):
-            for half in (0, 1):
-                j = ORDER[half][k]
-                sec, prim = self.at(half)
-                origin = ring(prim, STEPS[j])
-                for d, by in DIRS:
-                    self.wait(half, 12 + 2 * j + d, ring(sec, 2), origin, d * QUARTER, QUARTER)
+            self.arrived(6 + k, 4 * QUARTER)
+
+        def sent(self):
+            sent(self.buf.at[pl.ds(0, 15 * SHARD)], g_send.at[self.base])
 
     up_gather = Gather(up, up_all, 0)
-    down_gather = Gather(down, down_all, 40)
+    down_gather = Gather(down, down_all, 1)
     after = ((s + 1) % 16, t)
     tail = pl.ds(ROWS - WINDOW, WINDOW)
     halo_copies = [
@@ -199,28 +196,25 @@
 
     def w_relay(k, by):
         src = out_weight.at[pl.ds(k * HALF, HALF), w_cols(ring(y, 2), 0, 2 * FEATURES)]
-        return remote(src, w_pass.at[k], w_send.at[5 + k], w_recv.at[5 + k], y_next[by])
+        return remote(src, w_pass.at[k], w_send.at[0], w_recv.at[0], y_next[by])
 
     for k, by in DIRS:
         start(w_relay(k, by))
-    start(remote(out_weight.at[:, w_cols(y, 1 - c)], w_rows(y, c), w_send.at[0], w_recv.at[0], partner))
+    start(remote(out_weight.at[:, w_cols(y, 1 - c)], w_rows(y, c), w_send.at[1], w_recv.at[1], partner))
     for k, by in DIRS:
         for cc in (0, 1):
             start(remote(
                 out_weight.at[:, w_cols(ring(y, by), cc)], w_rows(y, c),
-                w_send.at[1 + 2 * k + cc], w_recv.at[1 + 2 * k + c], (s, ring(y, by) * 2 + cc),
+                w_send.at[1], w_recv.at[2 + k], (s, ring(y, by) * 2 + cc),
             ))
 
-    def w_arrived(index, ref):
-        remote(ref, ref, w_send.at[index], w_recv.at[index], partner).wait_recv()
-
     def w_pass_on():
+        arrived(w_pass, w_recv.at[0])
         for k, by in DIRS:
-            w_relay(k, by).wait_recv()
             for cc in (0, 1):
                 start(remote(
                     w_pass.at[k, :, pl.ds(cc * FEATURES, FEATURES)], w_rows(ring(y, -by), c, k * HALF, HALF),
-                    w_send.at[7 + 2 * k + cc], w_recv.at[7 + 2 * k + c], (s, ring(y, by) * 2 + cc),
+                    w_send.at[1], w_recv.at[4], (s, ring(y, by) * 2 + cc),
                 ))
 
     key_at = lax.broadcasted_iota(jnp.int32, (2 * WINDOW, 3 * WINDOW), 0)
@@ -260,8 +254,8 @@
         return att_all.at[pl.ds(pl.multiple_of(row, 32), count), pl.ds(FIRST[part], PART)]
 
     def att_copy(part, index, ref, target):
-        k = part * 8 + index
-        return remote(ref, ref, att_send.at[k], att_recv.at[k], target)
+        k = part * 7 + (0, 1, 2, 2, 3, 4, 5, 6)[index]
+        return remote(ref, ref, att_send.at[0], att_recv.at[k], target)
 
     def att_arrived(part, index, ref):
         att_copy(part, index, ref, partner).wait_recv()
@@ -291,19 +285,15 @@
             near_y = ring(y, -by)
             att_arrived(part, 5 + d, att_rows(near_y, 1 - c, part))
             if part == 0:
-                for cc in (0, 1):
-                    w_arrived(1 + 2 * d + cc, w_rows(near_y, cc))
+                arrived(w_rows(near_y, 0, 0, 2 * HEADS), w_recv.at[2 + d])
             mix(near_y, part, False)
 
     def mix_far(part):
         far = ring(y, 2)
-        for d, by in DIRS:
-            att_arrived(part, 2 + d, att_rows(far, c, part, d * HALF, HALF))
+        att_arrived(part, 2, att_rows(far, c, part))
         start(att_copy(part, 7, att_rows(far, c, part), partner))
         if part == 0:
-            for d, by in DIRS:
-                for cc in (0, 1):
-                    w_arrived(7 + 2 * d + cc, w_rows(far, cc, d * HALF, HALF))
+            arrived(w_rows(far, 0, 0, 2 * HEADS), w_recv.at[4])
         att_arrived(part, 7, att_rows(far, 1 - c, part))
         mix(far, part, False)
 
@@ -333,8 +323,8 @@
             squares[sq_rows, tokens] = dot(ones, high, ((1,), (1,))) + dot(ones, low, ((1,), (1,)))
 
     def x_copy(part, index, ref, target):
-        k = part * 10 + index
-        return remote(ref, ref, x_send.at[k], x_recv.at[k], target)
+        k = part * 7 + (0, 0, 1, 1, 2, 2, 3, 4, 5, 6)[index]
+        return remote(ref, ref, x_send.at[0], x_recv.at[k], target)
 
     def x_arrived(part, index, ref):
         x_copy(part, index, ref, partner).wait_recv()
@@ -345,19 +335,17 @@
             start(x_copy(part, 2 * second + d, x_block(y, c, part, quarter), y_next[by]))
 
     def x_pass(part):
+        x_arrived(part, 0, x_block(y, c, part))
         for d, by in DIRS:
-            ref = x_block(ring(y, -by), c, part, d)
-            x_arrived(part, d, ref)
-            start(x_copy(part, 4 + d, ref, y_next[by]))
+            start(x_copy(part, 4 + d, x_block(ring(y, -by), c, part, d), y_next[by]))
 
     def x_near(part):
+        x_arrived(part, 2, x_block(y, c, part))
         for d, by in DIRS:
-            x_arrived(part, 2 + d, x_block(ring(y, -by), c, part, 1 - d))
             start(x_copy(part, 7 + d, x_block(ring(y, -by), c, part), partner))
 
     def x_far(part):
-        for d, by in DIRS:
-            x_arrived(part, 4 + d, x_block(ring(y, 2), c, part, d))
+        x_arrived(part, 4, x_block(ring(y, 2), c, part))
         start(x_copy(part, 9, x_block(ring(y, 2), c, part), partner))
 
     def hide(yy, part, first=False, last=False):
@@ -394,7 +382,7 @@
     up_gather.second()
     for copy in locals_[4:]:
         copy.wait()
-    w_arrived(0, w_rows(y, 1 - c))
+    arrived(w_rows(y, 1 - c), w_recv.at[1])
     for part in (0, 1):
         att_arrived(part, 4, att_rows(y, 1 - c, part))
         mix(y, part, True)
@@ -418,12 +406,9 @@
     x_begin(1, False)
     x_begin(1, True)
     start(x_copy(1, 6, x_block(y, c, 1), partner))
-    sq_copies = []
     for k in range(1, 8):
         ref = squares.at[sq_rows]
-        copy = remote(ref, ref, sq_send.at[k - 1], sq_recv.at[k - 1], (s, (t + k) % 8))
-        start(copy)
-        sq_copies.append(copy)
+        start(remote(ref, ref, sq_send.at[0], sq_recv.at[0], (s, (t + k) % 8)))
     x_near(0)
     up_gather.forward(2)
     x_far(0)
@@ -485,7 +470,7 @@
             k = self.pair * 2 + part
             return remote(
                 partials.at[self.rows(), lanes(part)], paired.at[self.paired_rows(), lanes(part)],
-                pair_send.at[k], pair_recv.at[k], partner,
+                pair_send.at[0], pair_recv.at[k], partner,
             )
 
         def to_side(self, part):
@@ -493,16 +478,15 @@
             return remote(
                 partials.at[self.rows(), lanes(part)],
                 chained.at[pl.ds(pl.multiple_of(self.part * HALF, 32), HALF), lanes(part)],
-                side_send.at[k], side_recv.at[k], y_next[-1 if self.half == 0 else 1],
+                side_send.at[0], side_recv.at[k], y_next[-1 if self.half == 0 else 1],
             )
 
         def to_owner(self, part):
             index = (self.away // 2) * 4 + self.part
-            k = index * 2 + part
             return remote(
                 partials.at[self.rows(), lanes(part)],
                 final.at[pl.ds(pl.multiple_of(index * HALF, 32), HALF), lanes(part)],
-                owner_send.at[k], owner_recv.at[k], (s, ring(y, -self.away) * 2 + c),
+                owner_send.at[0], owner_recv.at[part], (s, ring(y, -self.away) * 2 + c),
             )
 
         def add(self, part, side):
@@ -581,6 +565,14 @@
     compute(groups[4])
     combine(groups[4])
     relay(groups[3])
+    for copy in halo_copies:
+        copy.wait_send()
+    sent(w_pass, w_send.at[0])
+    sent(w_all.at[pl.ds(0, 7 * HEADS)], w_send.at[1])
+    sent(att_all.at[pl.ds(0, 7 * HEADS)], att_send.at[0])
+    sent(x_all.at[pl.ds(0, 7 * PART)], x_send.at[0])
+    sent(squares.at[pl.ds(0, 56)], sq_send.at[0])
+    up_gather.sent()
     down_gather.forward(2)
     compute(groups[7])
     relay(groups[2])
@@ -604,9 +596,10 @@
     relay(groups[9])
     relay(groups[8])
     relay(groups[10])
-
-    for copy in sq_copies:
-        copy.wait_recv()
+    down_gather.sent()
+    sent(paired, pair_send.at[0])
+
+    arrived(squares.at[pl.ds(0, 56)], sq_recv.at[0])
     own = [Piece(half, 0, 0) for half in (0, 1, 0, 1)]
     for part, p in enumerate(own):
         p.part = part
@@ -620,9 +613,7 @@
     def _(part):
         for p in own:
             p.to_pair(part).wait_recv()
-            for away in (1, 3):
-                p.away = away
-                p.to_owner(part).wait_recv()
+        arrived(final.at[pl.ds(0, FEATURES)], owner_recv.at[part])
 
         @pl.loop(0, PART // 128)
         def _(i):
@@ -636,18 +627,8 @@
             total = total * (1.0 / (norm * (1.0 / D) + EPSILON))
             result[tokens, :] = (stream[tokens, :].astype(F32) + jnp.transpose(total)).astype(BF16)
 
-    for copy in pending:
-        copy.wait_send()
-    for part in (0, 1):
-        for k in range(16):
-            p = own[0]
-            p.pair = k
-            p.to_pair(part).wait_send()
-        for p in own:
-            p.to_side(part).wait_send()
-            for away in (1, 3):
-                p.away = away
-                p.to_owner(part).wait_send()
+    sent(chained, side_send.at[0])
+    sent(final, owner_send.at[0])
 
 
 def body(
@@ -685,9 +666,9 @@
             pltpu.VMEM((64, ROWS), F32),
             pltpu.SMEM((3,), F32),
             pltpu.VMEM((FEATURES,), BF16),
-            dma((9,)), dma((11,)), dma((11,)), dma((2,)), dma((2,)), dma((80,)), dma((80,)),
-            dma((16,)), dma((16,)), dma((20,)), dma((20,)), dma((7,)), dma((7,)),
-            dma((32,)), dma((32,)), dma((8,)), dma((8,)), dma((16,)), dma((16,)),
+            dma((9,)), dma((2,)), dma((5,)), dma((2,)), dma((2,)), dma((2,)), dma((20,)),
+            dma((1,)), dma((14,)), dma((1,)), dma((14,)), dma((1,)), dma((1,)),
+            dma((1,)), dma((32,)), dma((1,)), dma((8,)), dma((1,)), dma((2,)),
         ],
         compiler_params=pltpu.CompilerParams(
             collective_id=0, has_side_effects=True, vmem_limit_bytes=60 * 2**20

time: 120 us -> 117 us (0.975)
  Pallas kernels: 119 us -> 116 us
    pallas_call x1, Pallas kernels: 119 us -> 116 us  [body(): pl.pallas_call(kernel, out_shape=pltpu.VMEM((ROWS, FEATURES), BF16), in_s...]
where the time goes in v6:
time: 117 us
  Pallas kernels  116 us (99%)
    pallas_call x1, Pallas kernels, body(): pl.pallas_call(kernel, out_shape=pltpu.VMEM((ROWS, FEATURES), BF16), in_s...  116 us

profile of v6, /device:TPU:9, one launch (start us, length us, event | category | flops | bytes accessed | tf_op | source)
XLA Modules:
  0.0 116.9 jit_solution(12986914758208373131)
XLA Ops:
  0.0 116.0 %shard_map.91 = bf16[1024,384]{1,0:T(8,128)(2,1)S(1)} custom-call(bf16[192,1024]{1,0:T(8,128)(2,1)} %bitcast.5, bf16[64,1024]{1,0:T(8,128)(2,1)} %bitcast.6, bf16[64,1024]{1,0:T(8,128)(2,1)} %bitcast.7, f32[3]{0:T(128)} %sinks_in.1, bf16[192,3072]{1,0:T(8,128)(2,1)} %out_weight.1, bf16[1024,384]{1,0:T(8,128)(2,1)} %residual.1, bf16[384]{0:T(512)(128)(2,1)} %gains_in.1, ...), custom_call_target="tpu_custom_call" | custom-call | tf_op jit(solution)/shard_map/pallas_call | solution.py:640
  116.1 0.9 copy.11

commit v7 on v6

--- a/solution.py
+++ b/solution.py
@@ -79,8 +79,8 @@
     locals_ = [
         pltpu.make_async_copy(src, dst, local_sem.at[i])
         for i, (src, dst) in enumerate([
+            (up, up_all.at[pl.ds(pl.multiple_of(s * SHARD, SHARD), SHARD)]),
             (queries, q_v), (keys, k_v), (values, v_v), (sinks_in, sink), (gains_in, gain), (residual, res_v),
-            (up, up_all.at[pl.ds(pl.multiple_of(s * SHARD, SHARD), SHARD)]),
             (down, down_all.at[pl.ds(pl.multiple_of(s * SHARD, SHARD), SHARD)]),
             (out_weight.at[:, pl.ds(pl.multiple_of(t * FEATURES, 128), FEATURES)],
              w_all.at[pl.ds(pl.multiple_of(t * HEADS, HEADS), HEADS)]),
@@ -176,7 +176,7 @@
         def sent(self):
             sent(self.buf.at[pl.ds(0, 15 * SHARD)], g_send.at[self.base])
 
-    up_gather = Gather(up, up_all, 0)
+    up_gather = Gather(up_all.at[pl.ds(pl.multiple_of(s * SHARD, SHARD), SHARD)], up_all, 0)
     down_gather = Gather(down, down_all, 1)
     after = ((s + 1) % 16, t)
     tail = pl.ds(ROWS - WINDOW, WINDOW)
@@ -186,6 +186,7 @@
     ]
     for copy in halo_copies:
         start(copy)
+    locals_[0].wait()
     up_gather.first()
 
     def w_cols(yy, cc=0, count=FEATURES):
@@ -236,7 +237,7 @@
             att_all[rows, lanes] = output[:, g * WINDOW : (g + 1) * WINDOW]
 
     near = (key_at > query_at) & (key_at <= query_at + WINDOW)
-    for copy in locals_[:4]:
+    for copy in locals_[1:5]:
         copy.wait()
     sinks = jnp.concatenate([jnp.full((1, WINDOW), sink[g], F32) for g in range(3)], axis=1)
 
@@ -380,7 +381,7 @@
     start(att_copy(1, 4, att_rows(y, c, 1), partner))
     w_pass_on()
     up_gather.second()
-    for copy in locals_[4:]:
+    for copy in locals_[5:]:
         copy.wait()
     arrived(w_rows(y, 1 - c), w_recv.at[1])
     for part in (0, 1):

time: 117 us -> 117 us (level)
  no operation moved by 1% of the time
where the time goes in v7:
time: 117 us
  Pallas kernels  116 us (99%)
    pallas_call x1, Pallas kernels, body(): pl.pallas_call(kernel, out_shape=pltpu.VMEM((ROWS, FEATURES), BF16), in_s...  116 us

profile of v7, /device:TPU:9, one launch (start us, length us, event | category | flops | bytes accessed | tf_op | source)
XLA Modules:
  0.0 116.8 jit_solution(14251920323126675313)
XLA Ops:
  0.0 115.9 %shard_map.91 = bf16[1024,384]{1,0:T(8,128)(2,1)S(1)} custom-call(bf16[192,1024]{1,0:T(8,128)(2,1)} %bitcast.5, bf16[64,1024]{1,0:T(8,128)(2,1)} %bitcast.6, bf16[64,1024]{1,0:T(8,128)(2,1)} %bitcast.7, f32[3]{0:T(128)} %sinks_in.1, bf16[192,3072]{1,0:T(8,128)(2,1)} %out_weight.1, bf16[1024,384]{1,0:T(8,128)(2,1)} %residual.1, bf16[384]{0:T(512)(128)(2,1)} %gains_in.1, ...), custom_call_target="tpu_custom_call" | custom-call | tf_op jit(solution)/shard_map/pallas_call | solution.py:641
  115.9 0.9 copy.11
